TPU v7x, 256 devices: a 4x2x16 block of a 4x16x16 slice. The times are simulated.
256 devices in a mesh: grp: 2 (over y), kv: 16 (over z), tp: 8 (over x, core).
Axes of the slice: x: 4, y: 2, z: 16, core: 2. Of those that a mesh axis runs over, the one named last changes fastest.
The devices are a block of a 4x16x16 slice.
Arguments:
- tokens: bfloat16 [2048, 8, 4096], P('kv', 'grp'), parts along dimension 1, may hold values from -72 to 72
- lengths: int32 [8], P('grp'), parts along dimension 0, may hold values from 1 to 2048, 3072 in all
- chosen: int32 [8, 32, 32, 8], P('grp', 'tp', 'kv'), parts along dimension 0, may hold values from -1 to 31, as said below
- w_query: bfloat16 [4096, 2048], P(None, 'tp'), may hold values from -0.09375 to 0.09375
- w_key: bfloat16 [4096, 2048], P(None, 'tp'), may hold values from -0.09375 to 0.09375
- w_value: bfloat16 [4096, 2048], P(None, 'tp'), may hold values from -0.09375 to 0.09375
- w_gate: bfloat16 [4096, 2, 32], P(None, None, 'tp'), may hold values from -0.09375 to 0.09375
- pool_weights: float32 [2, 32, 64], replicated, may hold values from -1 to 1
- w_out: bfloat16 [2048, 4096], P(None, 'tp'), may hold values from -0.5 to 0.5
Outputs:
- mixed: bfloat16 [2048, 8, 4096], P(('kv', 'tp'), 'grp'), parts along dimension 1
There are 2 independent parts, one for each index of `grp`. A program takes and returns all parts, laid end to end along the dimension named above; an argument that names none is the same for every part. Nothing has to cross between parts.
Inputs may be any that keep to these rules, and one draw needn't show every extreme that they name: `chosen`: for query block b the live slots hold min(8, b+1) distinct blocks, all <= b, among them b, b-1 (when b >= 1) and 0; the other slots are -1.
All inputs are finite; a program needn't handle non-finite values.
Results may differ from a plain program's by a relative error of at most 0.014.
Values may be sent and summed in bfloat16 or wider, within the bound.
A program may use at most 128 MiB of HBM per device.

v0:
```python
from functools import partial

import jax
import jax.numpy as jnp
from jax import lax
from jax.sharding import PartitionSpec as P

HD = 64
QB = 64
L_CMP = 32


LOW_FILL = -1e30


def sent_together(arrays, axis, dim, along):
    ends, at = ([], 0)
    for a in arrays[:-1]:
        at += a.shape[along]
        ends.append(at)
    both = jnp.concatenate(arrays, axis=along)
    return tuple(jnp.split(lax.all_gather(both, axis, axis=dim, tiled=True), ends, axis=along))


def laid_out(tiles, dim):
    dims = list(tiles.shape[1:])
    dims[dim] *= tiles.shape[0]
    return jnp.moveaxis(tiles, 0, dim).reshape(dims)


def sent_to_all(x, axis):
    size = lax.axis_size(axis)
    return lax.all_to_all(jnp.broadcast_to(x[None], (size, *x.shape)), axis, 0, 0, tiled=True)


def gathered_copies(x, axis, dim):
    return laid_out(sent_to_all(x, axis), dim)


def pooled_blocks(key_rows, pool_weight):
    row_count, seq_count, head_count, head_dim = key_rows.shape
    grouped = key_rows.reshape(row_count // L_CMP, L_CMP, seq_count, head_count, head_dim)
    return (grouped * pool_weight[None, :, None, None, :]).sum(1).astype(jnp.bfloat16)


def pooled_attend(queries, key_pooled, val_pooled, query_pos, lengths):
    head_dim = queries.shape[-1]
    cmp_end = jnp.arange(key_pooled.shape[0]) * L_CMP + L_CMP - 1
    scores = jnp.einsum(
        "qshd,cshd->shqc", queries, key_pooled, preferred_element_type=jnp.float32
    ) * head_dim ** (-0.5)
    usable = (cmp_end[None, None, :] <= query_pos[None, :, None]) & (
        cmp_end[None, None, :] < lengths[:, None, None]
    )
    usable = usable[:, None]
    row_top = jnp.max(jnp.where(usable, scores, LOW_FILL), axis=-1, keepdims=True)
    weights = jnp.where(usable, jnp.exp(scores - row_top), 0.0)
    totals = jnp.sum(weights, axis=-1)
    gathered = jnp.einsum(
        "shqc,cshd->shqd",
        weights.astype(jnp.bfloat16),
        val_pooled,
        preferred_element_type=jnp.float32,
    )
    return gathered / jnp.where(totals > 0, totals, 1.0)[..., None]


def fold_step(running, key_piece, begin_row, queries, chosen, query_pos, lengths):
    maxima, totals, weighted = running
    piece_keys, piece_values = key_piece
    head_dim = queries.shape[-1]
    key_pos = jnp.arange(piece_keys.shape[0])
    key_blk = key_pos // QB
    picked = jnp.any(chosen[..., None] == key_blk, axis=3)
    picked = jnp.repeat(picked, QB, axis=2)
    usable = (
        picked
        & (key_pos[None, None, None, :] <= query_pos[None, None, :, None])
        & (key_pos[None, None, None, :] < lengths[:, None, None, None])
    )
    scores = jnp.einsum(
        "qshd,kshd->shqk", queries, piece_keys, preferred_element_type=jnp.float32
    ) * head_dim ** (-0.5)
    new_max = jnp.maximum(maxima, jnp.max(jnp.where(usable, scores, LOW_FILL), axis=-1))
    weights = jnp.where(usable, jnp.exp(scores - new_max[..., None]), 0.0)
    shrink = jnp.exp(maxima - new_max)
    totals = jnp.sum(weights, axis=-1)
    weighted = jnp.einsum(
        "shqk,kshd->shqd",
        weights.astype(jnp.bfloat16),
        piece_values,
        preferred_element_type=jnp.float32,
    )
    return (new_max, totals, weighted)


def body(tokens, lengths, chosen, w_query, w_key, w_value, w_gate, pool_weights, w_out):
    row_count, seq_count, model_width = tokens.shape
    head_count = w_query.shape[1] // HD
    query_pos = lax.axis_index("kv") * row_count + jnp.arange(row_count)
    flat_rows = tokens.reshape(row_count * seq_count, model_width)

    def project(weight):
        product = jnp.dot(flat_rows, weight, preferred_element_type=jnp.float32)
        return product.astype(jnp.bfloat16).reshape(row_count, seq_count, head_count, HD)

    queries = project(w_query)
    key_rows = project(w_key)
    value_rows = project(w_value)
    gate_values = jax.nn.sigmoid(
        jnp.dot(
            flat_rows,
            w_gate.reshape(model_width, 2 * head_count),
            preferred_element_type=jnp.float32,
        )
    )
    gate_values = gate_values.reshape(row_count, seq_count, 2, head_count)
    key_pooled, val_pooled = (
        lax.all_gather(pooled_blocks(key_rows, pool_weights[0]), "kv", axis=0, tiled=True),
        lax.all_gather(pooled_blocks(value_rows, pool_weights[1]), "kv", axis=0, tiled=True),
    )
    start_state = (
        jnp.full((seq_count, head_count, row_count), LOW_FILL, jnp.float32),
        jnp.zeros((seq_count, head_count, row_count), jnp.float32),
        jnp.zeros((seq_count, head_count, row_count, HD), jnp.float32),
    )
    step_fn = partial(
        fold_step, queries=queries, chosen=chosen, query_pos=query_pos, lengths=lengths
    )
    maxima, totals, weighted = step_fn(
        start_state, sent_together((key_rows, value_rows), "kv", 0, 1), jnp.int32(0)
    )
    picked_out = weighted / jnp.where(totals > 0, totals, 1.0)[..., None]
    pooled_out = pooled_attend(queries, key_pooled, val_pooled, query_pos, lengths)
    combined = gate_values[:, :, 0, :, None] * pooled_out.transpose(2, 0, 1, 3) + gate_values[
        :, :, 1, :, None
    ] * picked_out.transpose(2, 0, 1, 3)
    live = query_pos[:, None] < lengths[None, :]
    attended = (
        jnp.where(live[:, :, None, None], combined, 0.0)
        .astype(jnp.bfloat16)
        .reshape(row_count, seq_count, head_count * HD)
    )
    group_count = lax.axis_size("tp")
    all_heads = gathered_copies(attended, "tp", 2)
    group_width = head_count * HD
    col_width = w_out.shape[1]
    grouped_rows = all_heads.reshape(row_count * seq_count, group_count, group_width)
    grouped_weight = w_out.reshape(group_count, group_width, col_width)
    partial_cols = jnp.einsum(
        "rgk,gkc->rgc", grouped_rows, grouped_weight, preferred_element_type=jnp.float32
    )
    column_sum = jnp.sum(partial_cols.astype(jnp.bfloat16).astype(jnp.float32), axis=1)
    column_out = column_sum.astype(jnp.bfloat16).reshape(row_count, seq_count, col_width)
    return lax.all_to_all(column_out, "tp", split_axis=0, concat_axis=2, tiled=True)


def solution(mesh):
    placed = (
        P("kv", "grp", None),
        P("grp"),
        P("grp", "tp", "kv", None),
        P(None, "tp"),
        P(None, "tp"),
        P(None, "tp"),
        P(None, None, "tp"),
        P(),
        P(None, "tp"),
    )
    return jax.shard_map(
        body, mesh=mesh, in_specs=placed, out_specs=P(("kv", "tp"), "grp", None), check_vma=False
    )
```

profile of v0, /device:TPU:33, one launch (start us, length us, event | category | flops | bytes accessed | tf_op | source)
XLA Modules:
  0.0 253.4 jit_solution(7430744240340942174)
XLA Ops:
  6.6 7.1 %reshape.211 = bf16[512,4096]{1,0:T(8,128)(2,1)} reshape(bf16[128,4,4096]{2,1,0:T(4,128)(2,1)} %param.9) | data formatting | bytes 8388608 | tf_op jit(solution)/shard_map/reshape | solution.py:101
  13.6 4.2 %convolution_convert_fusion = bf16[512,256]{1,0:T(8,128)(2,1)S(1)} fusion(bf16[512,4096]{1,0:T(8,128)(2,1)} %reshape.211, bf16[4096,256]{1,0:T(8,128)(2,1)} %param.14), kind=kOutput, calls=%fused_computation.24 | convolution fusion | flops 1073872896 | bytes 6553600 | tf_op jit(solution)/shard_map/dot_general | solution.py:104
  18.4 1.2 convolution_convert_fusion.1
  20.6 1.1 copy.52
  21.7 1.8 pad_maximum_fusion
  23.6 1.5 reshape.221
  25.6 4.1 %convolution_convert_fusion.2 = bf16[512,256]{1,0:T(8,128)(2,1)S(1)} fusion(bf16[512,4096]{1,0:T(8,128)(2,1)} %reshape.211, bf16[4096,256]{1,0:T(8,128)(2,1)} %param.12), kind=kOutput, calls=%fused_computation.26 | convolution fusion | flops 1073872896 | bytes 6553600 | tf_op jit(solution)/shard_map/dot_general | solution.py:104
  30.8 1.5 copy.47
  32.2 3.4 %fusion.21 = f32[512,8]{0,1:T(8,128)S(1)} fusion(bf16[512,4096]{1,0:T(8,128)(2,1)} %reshape.211, bf16[4096,8]{0,1:T(8,128)(2,1)S(1)} %reshape.212), kind=kOutput, calls=%fused_computation.30 | convolution fusion | flops 33566720 | bytes 4276224 | tf_op jit(solution)/shard_map/dot_general | solution.py:111
  35.6 1.3 reshape.213
  37.0 1.9 slice_bitcast_fusion.1
  41.0 1.5 multiply_reduce_fusion
  42.6 49.0 %all_gather.10 = bf16[64,4,4,64]{3,2,1,0:T(4,128)(2,1)} all-gather(bf16[4,4,4,64]{3,2,1,0:T(4,128)(2,1)S(1)} %multiply_reduce_fusion), channel_id=1, replica_groups=mesh['grp'=2,'kv'=16,'tp'=8] {'kv'}, dimensions={0}, use_global_device_ids=true | all-gather | bytes 139264 | tf_op jit(solution)/shard_map/all_gather | solution.py:120
  91.8 24.2 %all_gather.9 = bf16[64,4,4,64]{3,2,1,0:T(4,128)(2,1)S(1)} all-gather(bf16[4,4,4,64]{3,2,1,0:T(4,128)(2,1)S(1)} %multiply_reduce_fusion.1), channel_id=1, replica_groups=mesh['grp'=2,'kv'=16,'tp'=8] {'kv'}, dimensions={0}, use_global_device_ids=true | all-gather | bytes 139264 | tf_op jit(solution)/shard_map/all_gather | solution.py:119
  118.5 42.0 %all-gather.2.cloned.1.call-done = bf16[2048,8,4,64]{0,3,2,1:T(8,128)(2,1)} async-done(((bf16[128,8,4,64]{0,3,2,1:T(8,128)(2,1)}), bf16[2048,8,4,64]{0,3,2,1:T(8,128)(2,1)}) %all-gather.2.cloned.1.call-update) | async-done | bytes 8388624 | tf_op jit(solution)/shard_map/all_gather | solution.py:22
  160.5 6.9 %select_reduce_fusion = (f32[4,4,128]{2,1,0:T(4,128)S(1)}, f32[4,4,128,2048]{3,2,1,0:T(8,128)S(1)}) fusion(pred[4,2048]{1,0:T(4,128)(4,1)S(1)} %iota_compare_fusion.1, pred[128,2048]{1,0:T(8,128)(4,1)S(1)} %iota_compare_fusion, pred[4,4,2,2048]{3,2,1,0:T(4,128)(4,1)S(1)} %compare_reduce_fusion, bf16[128,4,4,64]{0,3,2,1:T(8,128)(2,1)S(1)} %copy.47, ...), kind=kOutput, calls=%fused_computation.2 | convolution fusion | flops 557840384 | bytes 21577728 | tf_op jit(solution)/shard_map/qshd,kshd->shqk/dot_general | solution.py:81
  167.4 7.2 %fusion.2 = (f32[4,4,128]{2,1,0:T(4,128)S(1)}, bf16[4,4,128,2048]{3,2,1,0:T(8,128)(2,1)}) fusion(f32[4,4,128,2048]{3,2,1,0:T(8,128)S(1)} %get-tuple-element.12, f32[4,4,128]{2,1,0:T(4,128)S(1)} %broadcast_maximum_fusion, pred[4,2048]{1,0:T(4,128)(4,1)S(1)} %iota_compare_fusion.1, pred[128,2048]{1,0:T(8,128)(4,1)S(1)} %iota_compare_fusion, ...), kind=kLoop, calls=%fused_computation.5 | loop fusion | flops 29358080 | bytes 25518080 | tf_op jit(solution)/shard_map/reduce_sum | solution.py:87
  174.6 7.6 %fusion.25 = f32[128,4,4,64]{0,3,2,1:T(8,128)S(1)} fusion(bf16[4,4,128,2048]{3,2,1,0:T(8,128)(2,1)} %get-tuple-element.6, bf16[2048,8,4,64]{0,3,2,1:T(8,128)(2,1)} %all-gather.2.cloned.1.call-done, f32[128,4,4]{0,2,1:T(4,128)S(1)} %compare_select_fusion, f32[128,4,4]{0,2,1:T(4,128)S(1)} %copy.50), kind=kOutput, calls=%fused_computation.35 | convolution fusion | flops 537133056 | bytes 13123584 | tf_op jit(solution)/shard_map/shqk,kshd->shqd/dot_general | solution.py:88
  182.3 1.6 fusion.18
  184.6 40.5 %all_to_all.23 = bf16[8,128,4,256]{3,2,1,0:T(4,128)(2,1)} all-to-all(bf16[8,128,4,256]{3,2,1,0:T(4,128)(2,1)S(1)} %broadcast_in_dim.84), channel_id=1, replica_groups=mesh['grp'=2,'kv'=16,'tp'=8] {'tp'}, dimensions={0} | all-to-all | bytes 4194304 | tf_op jit(solution)/shard_map/all_to_all | solution.py:33
  225.1 4.0 %reshape_reshape.2 = bf16[512,8,256]{2,0,1:T(8,128)(2,1)} reshape(bf16[128,4,8,256]{3,1,0,2:T(4,128)(2,1)} %bitcast.70) | data formatting | bytes 4194304 | tf_op jit(solution)/shard_map/reshape;reshape | solution.py:148
  229.1 2.9 %convert_reduce_fusion = bf16[512,512]{1,0:T(8,128)(2,1)S(1)} fusion(bf16[512,8,256]{2,0,1:T(8,128)(2,1)} %reshape_reshape.2, bf16[8,256,512]{2,1,0:T(8,128)(2,1)S(1)} %bitcast.69), kind=kOutput, calls=%fused_computation.11 | convolution fusion | flops 1077673984 | bytes 4718592 | tf_op jit(solution)/shard_map/rgk,gkc->rgc/dot_general | solution.py:150
  232.1 12.8 %all_to_all.24 = bf16[128,4,512]{2,1,0:T(4,128)(2,1)S(1)} all-to-all(bf16[128,4,512]{2,1,0:T(4,128)(2,1)S(1)} %reshape.219), channel_id=1, replica_groups=mesh['grp'=2,'kv'=16,'tp'=8] {'tp'}, dimensions={0} | all-to-all | bytes 1048576 | tf_op jit(solution)/shard_map/all_to_all | solution.py:155
  245.4 1.2 reshape.222
  (50 shorter events, 9.1 us)
Async XLA Ops:
  6.5 222.6 %copy-start = (bf16[2048,512]{1,0:T(8,128)(2,1)S(1)}, bf16[2048,512]{1,0:T(8,128)(2,1)}, u32[]{:S(2)}) copy-start(bf16[2048,512]{1,0:T(8,128)(2,1)} %param.17) | copy-start | bytes 6291460
  6.6 153.9 %all-gather.2.cloned.1.call-start = ((), (), s32[]{:S(2)}) async-start(), calls=%async_computation.2 | async-start | bytes 8912896 | tf_op jit(solution)/shard_map/all_gather | solution.py:22
  13.6 4.3 %copy-start.1 = (bf16[512,4096]{1,0:T(8,128)(2,1)S(1)}, bf16[512,4096]{1,0:T(8,128)(2,1)}, u32[]{:S(2)}) copy-start(bf16[512,4096]{1,0:T(8,128)(2,1)} %reshape.211) | copy-start | bytes 12582916
  13.6 4.7 %copy-start.8 = (bf16[4096,256]{1,0:T(8,128)(2,1)S(1)}, bf16[4096,256]{1,0:T(8,128)(2,1)}, u32[]{:S(2)}) copy-start(bf16[4096,256]{1,0:T(8,128)(2,1)} %param.13) | copy-start | bytes 6291460
  19.6 5.9 %copy-start.4 = (bf16[4096,2,4]{0,2,1:T(4,128)(2,1)S(1)}, bf16[4096,2,4]{0,2,1:T(4,128)(2,1)}, u32[]{:S(2)}) copy-start(bf16[4096,2,4]{0,2,1:T(4,128)(2,1)} %param.15) | copy-start | bytes 196612
  29.7 11.3 %copy-start.5 = (f32[2,32,64]{2,1,0:T(8,128)S(1)}, f32[2,32,64]{2,1,0:T(8,128)}, u32[]{:S(2)}) copy-start(f32[2,32,64]{2,1,0:T(8,128)} %param.16) | copy-start | bytes 49156
  32.2 83.8 %copy-start.6 = (s32[4,4,2,8]{3,2,1,0:T(2,128)S(1)}, s32[4,4,2,8]{3,2,1,0:T(2,128)}, u32[]{:S(2)}) copy-start(s32[4,4,2,8]{3,2,1,0:T(2,128)} %param.11) | copy-start | bytes 3076
  32.2 84.6 %copy-start.7 = (s32[4]{0:T(128)S(1)}, s32[4]{0:T(128)}, u32[]{:S(2)}) copy-start(s32[4]{0:T(128)} %param.10) | copy-start | bytes 52
  117.4 0.8 copy-start.2
  174.6 7.6 %copy-start.3 = (bf16[64,4,4,64]{3,2,1,0:T(4,128)(2,1)S(1)}, bf16[64,4,4,64]{3,2,1,0:T(4,128)(2,1)}, u32[]{:S(2)}) copy-start(bf16[64,4,4,64]{3,2,1,0:T(4,128)(2,1)} %all_gather.10) | copy-start | bytes 393220
Sparse Core Ops, SparseCore 0:
  23.7 136.7 all-gather.1
where the time goes:
time: 254 us; the launch traced here: 253 us
  blocking collectives  127 us (50%)
  waiting for transfers between devices  42.1 us (17%)
  matrix products  32.2 us (13%)
  local copies, waits for them, and re-layouts  26.4 us (10%)
  between operations  13.7 us (5%)
  other arithmetic  12.5 us (5%)
    all_gather x1, blocking collectives, body(): lax.all_gather(pooled_blocks(value_rows, pool_weights[1]), 'kv', axis=0,...  49 us
    all_gather x1, waiting for transfers between devices, sent_together(): lax.all_gather(both, axis, axis=dim, tiled=True)  42 us
    all_to_all x1, blocking collectives, sent_to_all(): lax.all_to_all(jnp.broadcast_to(x[None], (size, *x.shape)), axis, 0, 0, t...  40.5 us
    all_gather x1, blocking collectives, body(): lax.all_gather(pooled_blocks(key_rows, pool_weights[0]), 'kv', axis=0, ti...  24.2 us
    all_to_all x1, blocking collectives, body(): lax.all_to_all(column_out, 'tp', split_axis=0, concat_axis=2, tiled=True)  12.8 us
    dot_general x3, matrix products, project(): product = jnp.dot(flat_rows, weight, preferred_element_type=jnp.float32)  9.61 us
    dot_general x1, matrix products, fold_step(): jnp.einsum('shqk,kshd->shqd', weights.astype(jnp.bfloat16), piece_values,...  7.62 us
    reduce_sum x1, other arithmetic, fold_step(): totals = jnp.sum(weights, axis=-1)  7.22 us
  transfers between devices with their start and end apart: 1, of which 1 were waited for; matrix products, arithmetic and copies ran while one was open for 8% of the time, Pallas kernels for 0%

commit v1 on v0

v1 whole, which is shorter than its diff:
```python
import jax
import jax.numpy as jnp
from jax import lax
from jax.experimental import pallas as pl
from jax.experimental.pallas import tpu as pltpu
from jax.sharding import PartitionSpec as P

HD = 64
QB = 64
L_CMP = 32
NEG = -1e30
BF = jnp.bfloat16
F32 = jnp.float32
MESH = pl.DeviceIdType.MESH

ROWS = 128
AUX = 16
MSG = 3 * HD + AUX
LAST = (15, 11, 7, 5)
PLACE = (
    (13, 9, 11, 15),
    (6, 4, 7, 5),
    (3, 4, 2, 12),
    (3, 1, 0, 2),
)
RANK_ORDER = (0, 1, 2, 3)
TILE = 256


def iota(shape, dim):
    return lax.broadcasted_iota(jnp.int32, shape, dim)


def nt(a, b):
    return lax.dot_general(a, b, (((1,), (1,)), ((), ())), preferred_element_type=F32)


def nn(a, b):
    return jnp.dot(a, b, preferred_element_type=F32)


def kernel(
    n_kv, n_tp, n_seq, n_head,
    tok_hbm, len_ref, chosen_rows, wq_hbm, wk_hbm, wv_hbm, wg_ref, pw_ref, wo_hbm,
    out_ref,
    tok, w_buf, wo, sel_t, send, recv, k_ext, q_ext, v_all, pool_in, o_stage, a_buf, x_buf, y_buf, o_buf,
    load_sem, q_send, q_recv, o_send, o_recv, g_send, g_recv, y_send, y_recv,
):
    me = lax.axis_index("kv")
    tp = lax.axis_index("tp")
    chips = n_tp // 2
    core = lax.rem(tp, 2)
    chip = tp // 2
    right = lax.rem(chip + 1, chips) * 2 + core
    left = lax.rem(chip + chips - 1, chips) * 2 + core
    far = lax.rem(chip + 2, chips) * 2 + core
    partner = chip * 2 + 1 - core

    barrier = pltpu.get_barrier_semaphore()
    for step in range(1, n_kv):
        pl.semaphore_signal(
            barrier, inc=1, device_id={"kv": lax.rem(me + step, n_kv)}, device_id_type=MESH
        )
    for step in range(1, n_tp):
        pl.semaphore_signal(
            barrier, inc=1, device_id={"tp": lax.rem(tp + step, n_tp)}, device_id_type=MESH
        )

    loads = [
        pltpu.make_async_copy(tok_hbm, tok, load_sem.at[0]),
        pltpu.make_async_copy(wk_hbm, w_buf.at[0], load_sem.at[1]),
        pltpu.make_async_copy(wv_hbm, w_buf.at[1], load_sem.at[2]),
        pltpu.make_async_copy(wq_hbm, w_buf.at[2], load_sem.at[3]),
        pltpu.make_async_copy(wo_hbm, wo, load_sem.at[4]),
    ]
    for copy in loads:
        copy.start()

    lens = [len_ref[s] for s in range(n_seq)]
    ranks = []
    for s in range(n_seq):
        rank = jnp.int32(0)
        for o in range(n_seq):
            if o != s:
                ahead = (lens[o] >= lens[s]) if o < s else (lens[o] > lens[s])
                rank = rank + ahead.astype(jnp.int32)
        ranks.append(rank)
    seq_of, len_of = [], []
    for r in range(n_seq):
        seq, length = jnp.int32(0), jnp.int32(0)
        for s in range(n_seq):
            hit = (ranks[s] == r).astype(jnp.int32)
            seq = seq + hit * s
            length = length + hit * lens[s]
        seq_of.append(seq)
        len_of.append(length)

    total = ROWS * n_seq
    row = iota((total, ROWS), 0)
    col = iota((total, ROWS), 1)
    for r in range(n_seq):
        hit = row == col * n_seq + seq_of[r]
        sel_t[:, r * ROWS : (r + 1) * ROWS] = jnp.where(hit, 1.0, 0.0).astype(BF)

    loads[0].wait()
    flat = tok[...].reshape(total, tok.shape[2])
    for part, slot, base in ((1, 0, HD), (2, 1, 2 * HD), (3, 2, 0)):
        loads[part].wait()
        made = nn(flat, w_buf[slot]).astype(BF).T
        placed = nn(made, sel_t[...])
        if base == 0:
            placed = placed * HD**-0.5
        placed = placed.astype(BF)
        for r in range(n_seq):
            for h in range(n_head):
                send[r * n_head + h, base : base + HD, :] = placed[
                    h * HD : (h + 1) * HD, r * ROWS : (r + 1) * ROWS
                ]
    gates = jax.nn.sigmoid(nt(flat, wg_ref[...]))
    gate_hi = gates.astype(BF)
    gate_lo = (gates - gate_hi.astype(F32)).astype(BF)
    gate_hi = nn(gate_hi.T, sel_t[...])
    gate_lo = nn(gate_lo.T, sel_t[...])
    for r in range(n_seq):
        cols = slice(r * ROWS, (r + 1) * ROWS)
        for h in range(n_head):
            picked = chosen_rows[seq_of[r], h]
            aux = jnp.concatenate(
                [
                    gate_hi[h : h + 1, cols],
                    gate_hi[n_head + h : n_head + h + 1, cols],
                    gate_lo[h : h + 1, cols],
                    gate_lo[n_head + h : n_head + h + 1, cols],
                    jnp.zeros((4, ROWS), F32),
                    picked,
                ],
                axis=0,
            )
            send[r * n_head + h, 3 * HD :, :] = aux.astype(BF)

    pl.semaphore_wait(barrier, n_kv - 1 + n_tp - 1)

    def message(r, h):
        return pltpu.make_async_remote_copy(
            src_ref=send.at[r * n_head + h],
            dst_ref=recv.at[r, me],
            send_sem=q_send.at[r * n_head + h],
            recv_sem=q_recv.at[r, me],
            device_id={"kv": jnp.int32(PLACE[r][h])},
            device_id_type=MESH,
        )

    def arrival(r, j):
        return pltpu.make_async_remote_copy(
            src_ref=send.at[0],
            dst_ref=recv.at[r, j],
            send_sem=q_send.at[0],
            recv_sem=q_recv.at[r, j],
            device_id={"kv": jnp.int32(0)},
            device_id_type=MESH,
        )

    for r in RANK_ORDER:
        for h in range(n_head):
            there = PLACE[r][h]

            @pl.when((me <= LAST[r]) & (me != there))
            def _():
                message(r, h).start()

            if there <= LAST[r]:

                @pl.when(me == there)
                def _():
                    recv[r, there] = send[r * n_head + h]

    def returned(r, h_here, j):
        return pltpu.make_async_remote_copy(
            src_ref=o_stage.at[r, j],
            dst_ref=a_buf.at[r, h_here],
            send_sem=o_send.at[r, j],
            recv_sem=o_recv.at[r, h_here],
            device_id={"kv": jnp.int32(j)},
            device_id_type=MESH,
        )

    def attend(r):
        shards = LAST[r] + 1
        span = shards * ROWS
        length = len_of[r]
        head = jnp.int32(0)
        for h in range(n_head):
            head = head + (me == PLACE[r][h]).astype(jnp.int32) * h

        pw_keys = jnp.concatenate([pw_ref[0].T] * (ROWS // L_CMP), axis=1)
        pw_vals = jnp.concatenate([pw_ref[1].T] * (ROWS // L_CMP), axis=1)
        weight = jnp.concatenate([pw_keys, pw_vals], axis=0)
        lane_blk = iota((ROWS, ROWS), 0) // L_CMP
        lane_col = iota((ROWS, ROWS), 1)

        def prepare(j, pooled):
            @pl.when(j != me)
            def _():
                arrival(r, j).wait_recv()

            cols = pl.ds(pl.multiple_of(j * ROWS, ROWS), ROWS)
            q_ext[0:HD, cols] = recv[r, j, 0:HD, :]
            k_ext[0:HD, cols] = recv[r, j, HD : 2 * HD, :]
            v_all[:, cols] = recv[r, j, 2 * HD : 3 * HD, :]
            picks = recv[r, j, 3 * HD : MSG, :].astype(F32)
            blocks = iota((32, ROWS), 0).astype(F32)
            hit = blocks == picks[8:9]
            for t in range(1, 8):
                hit = hit | (blocks == picks[8 + t : 9 + t])
            q_ext[HD : HD + 32, cols] = jnp.where(hit, 0.0, NEG).astype(BF)
            one_row = (iota((32, ROWS), 0) == 0).astype(F32)
            q_ext[HD + 32 :, cols] = one_row.astype(BF)
            key = j * ROWS + iota((32, ROWS), 1)
            k_ext[HD : HD + 32, cols] = (iota((32, ROWS), 0) == key // QB).astype(F32).astype(BF)
            k_ext[HD + 32 :, cols] = jnp.where(key >= length, one_row * NEG, 0.0).astype(BF)
            prod = recv[r, j, HD : 3 * HD, :].astype(F32) * weight
            hi = prod.astype(BF)
            lo = (prod - hi.astype(F32)).astype(BF)
            group = jnp.where(lane_col == j * (ROWS // L_CMP) + lane_blk, 1.0, 0.0).astype(BF)
            both = nn(jnp.concatenate([hi, lo], axis=0), group)
            return pooled + both[: 2 * HD] + both[2 * HD :]

        pooled = lax.fori_loop(0, shards, prepare, jnp.zeros((2 * HD, ROWS), F32)).astype(BF)
        key_pooled = jnp.concatenate([pooled[:HD], jnp.zeros((HD, ROWS), BF)], axis=0)
        val_pooled = pooled[HD:]
        for t in range(span // TILE):
            lo, hi = t * TILE, (t + 1) * TILE
            q = q_ext[:, lo:hi].T
            scores = nn(q, k_ext[:, :hi])
            edge = jnp.where(
                iota((TILE, TILE), 1) <= iota((TILE, TILE), 0), scores[:, lo:hi], NEG
            )
            scores = edge if t == 0 else jnp.concatenate([scores[:, :lo], edge], axis=1)
            top = jnp.max(scores, axis=1, keepdims=True)
            e = jnp.exp(scores - top)
            tot = jnp.sum(e, axis=1, keepdims=True)
            picked_out = nt(e.astype(BF), v_all[:, :hi]) / tot

            scores = nn(q, key_pooled)
            pos = lo + iota((TILE, ROWS), 0)
            end = iota((TILE, ROWS), 1) * L_CMP + (L_CMP - 1)
            usable = (end <= pos) & (end < length)
            top = jnp.max(jnp.where(usable, scores, NEG), axis=1, keepdims=True)
            e = jnp.where(usable, jnp.exp(jnp.where(usable, scores, NEG) - top), 0.0)
            tot = jnp.sum(e, axis=1, keepdims=True)
            pooled_out = nt(e.astype(BF), val_pooled) / jnp.where(tot > 0, tot, 1.0)

            both = jnp.concatenate([pooled_out, picked_out], axis=1).T
            for i in range(TILE // ROWS):
                j = t * (TILE // ROWS) + i
                g = recv[r, j, 3 * HD : MSG, :].astype(F32)
                part = both[:, i * ROWS : (i + 1) * ROWS]
                mix = (g[0:1] + g[2:3]) * part[:HD] + (g[1:2] + g[3:4]) * part[HD:]
                alive = j * ROWS + iota((HD, ROWS), 1) < length
                o_stage[r, j] = jnp.where(alive, mix, 0.0).astype(BF)

                @pl.when(me != j)
                def _():
                    returned(r, head, j).start()

                @pl.when(me == j)
                def _():
                    a_buf[r, head] = o_stage[r, j]

    def placed_here(r):
        here = me == PLACE[r][0]
        for h in range(1, n_head):
            here = here | (me == PLACE[r][h])
        return here

    for r in RANK_ORDER:

        @pl.when(placed_here(r))
        def _():
            attend(r)

    half = ROWS // 2
    lower, upper = pl.ds(0, half), pl.ds(half, half)

    def hop(r, block, rows, to, n):
        ref = x_buf.at[r, block] if rows is None else x_buf.at[r, block, rows]
        return pltpu.make_async_remote_copy(
            src_ref=ref,
            dst_ref=ref,
            send_sem=g_send.at[r, n],
            recv_sem=g_recv.at[r, n],
            device_id={"tp": to},
            device_id_type=MESH,
        )

    def sends(r):
        return [
            hop(r, tp, lower, right, 0),
            hop(r, tp, upper, right, 1),
            hop(r, tp, upper, left, 2),
            hop(r, tp, lower, left, 3),
            hop(r, left, lower, right, 4),
            hop(r, right, upper, left, 5),
            hop(r, tp, None, partner, 6),
            hop(r, left, None, partner, 7),
            hop(r, right, None, partner, 8),
            hop(r, far, None, partner, 9),
        ]

    def other(t):
        return t + 1 - 2 * lax.rem(t, 2)

    def receipts(r):
        return [
            hop(r, left, lower, left, 0),
            hop(r, left, upper, left, 1),
            hop(r, right, upper, right, 2),
            hop(r, right, lower, right, 3),
            hop(r, far, lower, left, 4),
            hop(r, far, upper, right, 5),
            hop(r, other(tp), None, partner, 6),
            hop(r, other(left), None, partner, 7),
            hop(r, other(right), None, partner, 8),
            hop(r, other(far), None, partner, 9),
        ]

    rows_each = ROWS // n_tp
    width = wo.shape[1]

    def column_copy(r, to):
        return pltpu.make_async_remote_copy(
            src_ref=y_buf.at[r, pl.ds(pl.multiple_of(to * rows_each, rows_each), rows_each)],
            dst_ref=o_buf.at[r, :, pl.ds(pl.multiple_of(tp * width, width), width)],
            send_sem=y_send.at[r, to],
            recv_sem=y_recv.at[r, tp],
            device_id={"tp": to},
            device_id_type=MESH,
        )

    def column_arrival(r, source):
        return pltpu.make_async_remote_copy(
            src_ref=y_buf.at[r, pl.ds(0, rows_each)],
            dst_ref=o_buf.at[r, :, pl.ds(pl.multiple_of(source * width, width), width)],
            send_sem=y_send.at[r, source],
            recv_sem=y_recv.at[r, source],
            device_id={"tp": source},
            device_id_type=MESH,
        )

    loads[4].wait()

    def spread(r):
        for h in range(n_head):

            @pl.when(me != PLACE[r][h])
            def _():
                pltpu.make_async_remote_copy(
                    src_ref=o_stage.at[r, 0],
                    dst_ref=a_buf.at[r, h],
                    send_sem=o_send.at[r, 0],
                    recv_sem=o_recv.at[r, h],
                    device_id={"kv": jnp.int32(PLACE[r][h])},
                    device_id_type=MESH,
                ).wait_recv()

        x_buf[r, tp] = a_buf[r].reshape(n_head * HD, ROWS).T
        out, into = sends(r), receipts(r)
        for n in (0, 2, 1, 3, 6):
            out[n].start()
        into[0].wait_recv()
        out[4].start()
        into[2].wait_recv()
        out[5].start()
        into[1].wait_recv()
        out[7].start()
        into[3].wait_recv()
        out[8].start()
        into[4].wait_recv()
        into[5].wait_recv()
        out[9].start()
        for n in (6, 7, 8, 9):
            into[n].wait_recv()
        rows = jnp.concatenate([x_buf[r, g] for g in range(n_tp)], axis=1)
        y_buf[r] = nn(rows, wo[...]).astype(BF)
        for step in range(1, n_tp):
            column_copy(r, lax.rem(tp + step, n_tp)).start()
        mine = pl.ds(pl.multiple_of(tp * rows_each, rows_each), rows_each)
        o_buf[r, :, pl.ds(pl.multiple_of(tp * width, width), width)] = y_buf[r, mine]

    for r in RANK_ORDER:

        @pl.when(me <= LAST[r])
        def _():
            spread(r)

        @pl.when(me > LAST[r])
        def _():
            o_buf[r] = jnp.zeros(o_buf.shape[1:], BF)

    for r in range(n_seq):

        @pl.when(me <= LAST[r])
        def _():
            for step in range(1, n_tp):
                column_arrival(r, lax.rem(tp + step, n_tp)).wait_recv()

    many = rows_each * n_seq
    want = iota((many, many), 0)
    have = iota((many, many), 1)
    pick = jnp.zeros((many, many), F32)
    for r in range(n_seq):
        hit = (have == r * rows_each + want // n_seq) & (lax.rem(want, n_seq) == seq_of[r])
        pick = jnp.where(hit, 1.0, pick)
    pick = pick.astype(BF)
    for c in range(n_tp):
        cols = slice(c * width, (c + 1) * width)
        rows = o_buf[:, :, cols].reshape(many, width)
        out_ref[:, cols] = nn(pick, rows).astype(BF)

    for r in range(n_seq):
        for h in range(n_head):

            @pl.when((me <= LAST[r]) & (me != PLACE[r][h]))
            def _():
                message(r, h).wait_send()

        @pl.when(placed_here(r))
        def _():
            for j in range(LAST[r] + 1):

                @pl.when(me != j)
                def _():
                    returned(r, 0, j).wait_send()

        @pl.when(me <= LAST[r])
        def _():
            for copy in sends(r):
                copy.wait_send()
            for step in range(1, n_tp):
                column_copy(r, lax.rem(tp + step, n_tp)).wait_send()


def body(tokens, lengths, chosen, w_query, w_key, w_value, w_gate, pool_weights, w_out):
    rows, n_seq, depth = tokens.shape
    n_head = w_query.shape[1] // HD
    n_kv, n_tp = lax.axis_size("kv"), lax.axis_size("tp")
    blocks = chosen.shape[2]
    picks = jnp.repeat(jnp.swapaxes(chosen, 2, 3), rows // blocks, axis=3).astype(F32)
    gate_rows = jnp.transpose(w_gate, (1, 2, 0)).reshape(2 * n_head, depth)
    width = w_out.shape[1]
    total = rows * n_seq
    vmem = pl.BlockSpec(memory_space=pltpu.VMEM)
    hbm = pl.BlockSpec(memory_space=pl.ANY)
    dma = pltpu.SemaphoreType.DMA
    full = n_kv * rows

    def whole(*refs):
        kernel(n_kv, n_tp, n_seq, n_head, *refs)

    out = pl.pallas_call(
        whole,
        out_shape=jax.ShapeDtypeStruct((total // n_tp, n_tp * width), BF),
        in_specs=[
            hbm, pl.BlockSpec(memory_space=pltpu.SMEM), vmem, hbm, hbm, hbm, vmem, vmem, hbm,
        ],
        out_specs=vmem,
        scratch_shapes=[
            pltpu.VMEM((rows, n_seq, depth), BF),
            pltpu.VMEM((3, depth, n_head * HD), BF),
            pltpu.VMEM(w_out.shape, BF),
            pltpu.VMEM((total, total), BF),
            pltpu.VMEM((n_seq * n_head, MSG, rows), BF),
            pltpu.VMEM((n_seq, n_kv, MSG, rows), BF),
            pltpu.VMEM((128, full), BF),
            pltpu.VMEM((128, full), BF),
            pltpu.VMEM((HD, full), BF),
            pltpu.VMEM((8, 128), F32),
            pltpu.VMEM((n_seq, n_kv, HD, rows), BF),
            pltpu.VMEM((n_seq, n_head, HD, rows), BF),
            pltpu.VMEM((n_seq, n_tp, rows, n_head * HD), BF),
            pltpu.VMEM((n_seq, rows, width), BF),
            pltpu.VMEM((n_seq, rows // n_tp, n_tp * width), BF),
            dma((5,)),
            dma((n_seq * n_head,)),
            dma((n_seq, n_kv)),
            dma((n_seq, n_kv)),
            dma((n_seq, n_head)),
            dma((n_seq, 10)),
            dma((n_seq, 10)),
            dma((n_seq, n_tp)),
            dma((n_seq, n_tp)),
        ],
        compiler_params=pltpu.CompilerParams(
            collective_id=0, has_side_effects=True, vmem_limit_bytes=60 * 2**20
        ),
    )(tokens, lengths, picks, w_query, w_key, w_value, gate_rows, pool_weights, w_out)
    return out.reshape(rows // n_tp, n_seq, n_tp * width)


def solution(mesh):
    placed = (
        P("kv", "grp", None),
        P("grp"),
        P("grp", "tp", "kv", None),
        P(None, "tp"),
        P(None, "tp"),
        P(None, "tp"),
        P(None, None, "tp"),
        P(),
        P(None, "tp"),
    )
    return jax.shard_map(
        body, mesh=mesh, in_specs=placed, out_specs=P(("kv", "tp"), "grp", None), check_vma=False
    )
```

time: 254 us -> 115 us (0.45)
  blocking collectives: 127 us -> 0 us
  Pallas kernels: 0 us -> 109 us
  waiting for transfers between devices: 42.1 us -> 0 us
  matrix products: 32.2 us -> 0 us
  local copies, waits for them, and re-layouts: 26.4 us -> 4.63 us
  between operations: 13.7 us -> 0.02 us
  other arithmetic: 12.5 us -> 0.72 us
    pallas_call x0 -> x1, Pallas kernels: none -> 109 us  [body(): pl.pallas_call(whole, out_shape=jax.ShapeDtypeStruct((total // n_tp, n_tp...]
    all_gather x2 -> x0, blocking collectives: 73.2 us -> none  [the longest x1 49 us: body(): lax.all_gather(pooled_blocks(value_rows, pool_weights[1]), 'kv', axis=0,...]
    all_to_all x2 -> x0, blocking collectives: 53.3 us -> none  [the longest x1 40.5 us: sent_to_all(): lax.all_to_all(jnp.broadcast_to(x[None], (size, *x.shape)), axis, 0, 0, t...]
    all_gather x1 -> x0, waiting for transfers between devices: 42 us -> none  [sent_together(): lax.all_gather(both, axis, axis=dim, tiled=True)]
    dot_general x9 -> x0, matrix products: 32.2 us -> none  [the longest x3 9.61 us: project(): product = jnp.dot(flat_rows, weight, preferred_element_type=jnp.float32)]
    reshape x10 -> x2, local copies, waits for them, and re-layouts: 13.1 us -> 3.51 us  [the longest x1 2.03 us: body(): return out.reshape(rows // n_tp, n_seq, n_tp * width)]
    reduce_sum x3 -> x0, other arithmetic: 9.02 us -> none  [the longest x1 7.22 us: fold_step(): totals = jnp.sum(weights, axis=-1)]
    mul x4 -> x0, local copies, waits for them, and re-layouts: 4.04 us -> none  [the longest x2 2.97 us: body(): gate_values[:, :, 0, :, None] * pooled_out.transpose(2, 0, 1, 3)]
  transfers between devices with their start and end apart: 1 -> 0, of which waited for: 1 -> 0; matrix products, arithmetic and copies ran while one was open for 8% -> 0% of each run, Pallas kernels for 0% -> 0%
where the time goes in v1:
time: 115 us
  Pallas kernels  109 us (95%)
  local copies, waits for them, and re-layouts  4.63 us (4%)
    pallas_call x1, Pallas kernels, body(): pl.pallas_call(whole, out_shape=jax.ShapeDtypeStruct((total // n_tp, n_tp...  109 us

profile of v1, /device:TPU:33, one launch (start us, length us, event | category | flops | bytes accessed | tf_op | source)
XLA Modules:
  0.0 114.9 jit_solution(7375409172821631018)
XLA Ops:
  0.0 0.7 convert_bitcast_fusion
  0.7 0.2 copy.10
  0.9 0.2 broadcast_in_dim.3
  1.1 0.8 convert_element_type.9.refs_2_
  1.9 1.5 %reshape.8.refs_6_ = bf16[8,4096]{1,0:T(8,128)(2,1)} reshape(bf16[2,4,4096]{2,1,0:T(4,128)(2,1)} %bitcast.3) | data formatting | bytes 131072 | tf_op jit(solution)/shard_map/reshape | solution.py:449
  3.3 109.5 %shard_map.91 = bf16[64,4096]{1,0:T(8,128)(2,1)} custom-call(bf16[128,4,4096]{2,1,0:T(4,128)(2,1)} %refs_0_.1, s32[4]{0:T(128)} %refs_1_.1, f32[4,4,8,128]{3,2,1,0:T(8,128)} %convert_element_type.9.refs_2_, bf16[4096,256]{1,0:T(8,128)(2,1)} %refs_3_.1, bf16[4096,256]{1,0:T(8,128)(2,1)} %refs_4_.1, bf16[4096,256]{1,0:T(8,128)(2,1)} %refs_5_.1, ...), custom_call_target="tpu_custom_call" | custom-call | tf_op jit(solution)/shard_map/pallas_call | solution.py:460
  112.8 2.0 %reshape.9 = bf16[16,4,4096]{2,1,0:T(4,128)(2,1)} reshape(bf16[64,4096]{1,0:T(8,128)(2,1)} %shard_map.91) | data formatting | bytes 1048576 | tf_op jit(solution)/shard_map/reshape | solution.py:497

commit v2 on v1

v2 whole, which is shorter than its diff:
```python
import jax
import jax.numpy as jnp
from jax import lax
from jax.experimental import pallas as pl
from jax.experimental.pallas import tpu as pltpu
from jax.sharding import PartitionSpec as P

HD = 64
QB = 64
L_CMP = 32
NEG = -1e30
BF = jnp.bfloat16
F32 = jnp.float32
MESH = pl.DeviceIdType.MESH

ROWS = 128
AUX = 16
MSG = 3 * HD + AUX
KEYS, VALS, QUER, EXTRA = 0, HD, 2 * HD, 3 * HD
LAST = (15, 11, 7, 5)
PLACE = (
    (9, 11, 12, 13),
    (4, 5, 6, 7),
    (3, 4, 1, 2),
    (2, 3, 1, 5),
)
RANK_ORDER = (3, 2, 1, 0)
TILE = 256
SHARDS = LAST[0] + 1
PAIRED = sorted({p for places in PLACE for p in places})


def returns_to(i, j):
    return any(i in PLACE[r] and j <= LAST[r] for r in range(len(PLACE)))


def sends_to(i, j):
    asked = any(j in PLACE[r] and i <= LAST[r] for r in range(len(PLACE)))
    return asked or returns_to(i, j)


def any_of(me, places):
    here = me < 0
    for p in places:
        here = here | (me == p)
    return here


def iota(shape, dim):
    return lax.broadcasted_iota(jnp.int32, shape, dim)


def nt(a, b):
    return lax.dot_general(a, b, (((1,), (1,)), ((), ())), preferred_element_type=F32)


def nn(a, b):
    return jnp.dot(a, b, preferred_element_type=F32)


def kernel(
    n_kv, n_tp, n_seq, n_head,
    tok_hbm, len_hbm, chosen_hbm, wq_hbm, wk_hbm, wv_hbm, wg_hbm, pw_hbm, wo_hbm,
    out_ref,
    tok, flat, w_buf, wg, pw_ref, wo, len_ref, chosen_ref,
    sel_t, send, recv, k_ext, q_ext, v_all, weight, pool_sum, o_stage, a_buf, x_buf, y_buf, o_buf,
    load_sem, k_send, k_recv, q_send, q_recv, o_send, o_recv, g_send, g_recv, y_send, y_recv,
    ready_kv, ready_tp,
):
    me = lax.axis_index("kv")
    tp = lax.axis_index("tp")
    chips = n_tp // 2
    core = lax.rem(tp, 2)
    chip = tp // 2
    right = lax.rem(chip + 1, chips) * 2 + core
    left = lax.rem(chip + chips - 1, chips) * 2 + core
    far = lax.rem(chip + 2, chips) * 2 + core
    partner = chip * 2 + 1 - core

    barrier = pltpu.get_barrier_semaphore()
    for j in range(n_kv):

        @pl.when(me < j)
        def _():
            pl.semaphore_signal(
                barrier, inc=1, device_id={"kv": jnp.int32(j)}, device_id_type=MESH
            )

    for t in range(n_tp):

        @pl.when(tp > t)
        def _():
            pl.semaphore_signal(
                barrier, inc=1, device_id={"tp": jnp.int32(t)}, device_id_type=MESH
            )

    loads = [
        pltpu.make_async_copy(len_hbm, len_ref, load_sem.at[0]),
        pltpu.make_async_copy(tok_hbm, tok, load_sem.at[1]),
        pltpu.make_async_copy(wk_hbm, w_buf.at[0], load_sem.at[2]),
        pltpu.make_async_copy(wv_hbm, w_buf.at[1], load_sem.at[3]),
        pltpu.make_async_copy(wq_hbm, w_buf.at[2], load_sem.at[4]),
        pltpu.make_async_copy(wg_hbm, wg, load_sem.at[5]),
        pltpu.make_async_copy(chosen_hbm, chosen_ref, load_sem.at[6]),
        pltpu.make_async_copy(pw_hbm, pw_ref, load_sem.at[7]),
        pltpu.make_async_copy(wo_hbm, wo, load_sem.at[8]),
    ]
    for copy in loads:
        copy.start()
    told = me + n_tp - 1 - tp

    @pl.when(told > 0)
    def _():
        pl.semaphore_wait(barrier, told)

    for i in range(n_kv):
        later = [j for j in range(i + 1, n_kv) if sends_to(i, j)]

        @pl.when(any_of(me, later))
        def _():
            pl.semaphore_signal(
                ready_kv.at[me], inc=1, device_id={"kv": jnp.int32(i)}, device_id_type=MESH
            )

    for t in range(n_tp):

        @pl.when(tp < t)
        def _():
            pl.semaphore_signal(
                ready_tp.at[tp], inc=1, device_id={"tp": jnp.int32(t)}, device_id_type=MESH
            )

    loads[0].wait()

    lens = [len_ref[s] for s in range(n_seq)]
    ranks = []
    for s in range(n_seq):
        rank = jnp.int32(0)
        for o in range(n_seq):
            if o != s:
                ahead = (lens[o] >= lens[s]) if o < s else (lens[o] > lens[s])
                rank = rank + ahead.astype(jnp.int32)
        ranks.append(rank)
    seq_of, len_of = [], []
    for r in range(n_seq):
        seq, length = jnp.int32(0), jnp.int32(0)
        for s in range(n_seq):
            hit = (ranks[s] == r).astype(jnp.int32)
            seq = seq + hit * s
            length = length + hit * lens[s]
        seq_of.append(seq)
        len_of.append(length)

    total = ROWS * n_seq
    row = iota((total, ROWS), 0)
    col = iota((total, ROWS), 1)
    for r in range(n_seq):
        hit = row == col * n_seq + seq_of[r]
        sel_t[:, r * ROWS : (r + 1) * ROWS] = jnp.where(hit, 1.0, 0.0).astype(BF)

    loads[1].wait()
    flat[...] = tok[...].reshape(flat.shape)

    def project(slot, base):
        loads[2 + slot].wait()
        made = nn(flat[...], w_buf[slot]).astype(BF).T
        placed = nn(made, sel_t[...])
        if base == QUER:
            placed = placed * HD**-0.5
        placed = placed.astype(BF)
        for r in range(n_seq):
            for h in range(n_head):
                send[r * n_head + h, base : base + HD, :] = placed[
                    h * HD : (h + 1) * HD, r * ROWS : (r + 1) * ROWS
                ]

    def extras():
        loads[5].wait()
        loads[6].wait()
        gates = jax.nn.sigmoid(nt(wg[...].reshape(2 * n_head, wg.shape[2]), flat[...]))
        gate_hi = gates.astype(BF)
        gate_lo = (gates - gate_hi.astype(F32)).astype(BF)
        gate_rows = nn(jnp.concatenate([gate_hi, gate_lo], axis=0), sel_t[...])
        n_blk, top = chosen_ref.shape[2:]
        slot = iota((top, ROWS), 0)
        blk = iota((top, ROWS), 1) // (ROWS // n_blk)
        for r in range(n_seq):
            cols = slice(r * ROWS, (r + 1) * ROWS)
            for h in range(n_head):
                picked = jnp.zeros((top, ROWS), jnp.int32)
                for b in range(n_blk):
                    for t in range(top):
                        at = (slot == t) & (blk == b)
                        picked = jnp.where(at, chosen_ref[seq_of[r], h, b, t], picked)
                kinds = [
                    gate_rows[g * n_head + h : g * n_head + h + 1, cols] for g in range(4)
                ]
                rest = jnp.zeros((AUX - top - 4, ROWS), F32)
                aux = jnp.concatenate([*kinds, rest, picked.astype(F32)], axis=0)
                send[r * n_head + h, EXTRA:, :] = aux.astype(BF)

    pair_rows = pl.ds(0, QUER)
    query_rows = pl.ds(QUER, MSG - QUER)

    def message(r, h, queries):
        rows = query_rows if queries else pair_rows
        return pltpu.make_async_remote_copy(
            src_ref=send.at[r * n_head + h, rows],
            dst_ref=recv.at[r, me, rows],
            send_sem=(q_send if queries else k_send).at[r * n_head + h],
            recv_sem=(q_recv if queries else k_recv).at[r, me],
            device_id={"kv": jnp.int32(PLACE[r][h])},
            device_id_type=MESH,
        )

    def arrival(r, j, queries):
        rows = query_rows if queries else pair_rows
        return pltpu.make_async_remote_copy(
            src_ref=send.at[0, rows],
            dst_ref=recv.at[r, j, rows],
            send_sem=(q_send if queries else k_send).at[0],
            recv_sem=(q_recv if queries else k_recv).at[r, j],
            device_id={"kv": jnp.int32(0)},
            device_id_type=MESH,
        )

    asked = set()

    def send_rank(r, queries):
        for h in range(n_head):
            there = PLACE[r][h]
            if there not in asked:
                asked.add(there)

                @pl.when(any_of(me, [i for i in range(there) if sends_to(i, there)]))
                def _():
                    pl.semaphore_wait(ready_kv.at[there], 1)

            @pl.when((me <= LAST[r]) & (me != there))
            def _():
                message(r, h, queries).start()

            if queries and there <= LAST[r]:

                @pl.when(me == there)
                def _():
                    recv[r, there] = send[r * n_head + h]

    project(0, KEYS)
    project(1, VALS)
    for r in RANK_ORDER[:2]:
        send_rank(r, False)
    project(2, QUER)
    extras()
    for r in RANK_ORDER[:2]:
        send_rank(r, True)
    for r in RANK_ORDER[2:]:
        send_rank(r, False)
        send_rank(r, True)
    loads[7].wait()

    def returned(r, h_here, j):
        return pltpu.make_async_remote_copy(
            src_ref=o_stage.at[r, j],
            dst_ref=a_buf.at[r, h_here],
            send_sem=o_send.at[r, j],
            recv_sem=o_recv.at[r, h_here],
            device_id={"kv": jnp.int32(j)},
            device_id_type=MESH,
        )

    def attend(r):
        shards = LAST[r] + 1
        span = shards * ROWS
        length = len_of[r]
        head = jnp.int32(0)
        for h in range(n_head):
            head = head + (me == PLACE[r][h]).astype(jnp.int32) * h

        pw_keys = jnp.concatenate([pw_ref[0].T] * (ROWS // L_CMP), axis=1)
        pw_vals = jnp.concatenate([pw_ref[1].T] * (ROWS // L_CMP), axis=1)
        weight[...] = jnp.concatenate([pw_keys, pw_vals], axis=0)
        lane_blk = iota((ROWS, ROWS), 0) // L_CMP
        lane_col = iota((ROWS, ROWS), 1)

        def prepare(j):
            @pl.when(me != j)
            def _():
                arrival(r, j, False).wait_recv()
                arrival(r, j, True).wait_recv()

            cols = slice(j * ROWS, (j + 1) * ROWS)
            q_ext[0:HD, cols] = recv[r, j, QUER:EXTRA, :]
            k_ext[0:HD, cols] = recv[r, j, KEYS:VALS, :]
            v_all[0:HD, cols] = recv[r, j, VALS:QUER, :]
            picks = recv[r, j, EXTRA:MSG, :].astype(F32)
            blocks = iota((32, ROWS), 0).astype(F32)
            hit = blocks == picks[8:9]
            for t in range(1, 8):
                hit = hit | (blocks == picks[8 + t : 9 + t])
            q_ext[HD : HD + 32, cols] = jnp.where(hit, 0.0, NEG).astype(BF)
            one_row = (iota((32, ROWS), 0) == 0).astype(F32)
            q_ext[HD + 32 :, cols] = one_row.astype(BF)
            key = j * ROWS + iota((32, ROWS), 1)
            k_ext[HD : HD + 32, cols] = (iota((32, ROWS), 0) == key // QB).astype(F32).astype(BF)
            k_ext[HD + 32 :, cols] = jnp.where(key >= length, one_row * NEG, 0.0).astype(BF)
            v_all[HD:, cols] = (iota((HD, ROWS), 0) == 0).astype(F32).astype(BF)
            prod = recv[r, j, KEYS:QUER, :].astype(F32) * weight[...]
            hi = prod.astype(BF)
            lo = (prod - hi.astype(F32)).astype(BF)
            group = jnp.where(lane_col == j * (ROWS // L_CMP) + lane_blk, 1.0, 0.0).astype(BF)
            return [hi, lo], [group, group]

        pool_sum[...] = jnp.zeros((2 * HD, ROWS), F32)
        for t in range(span // TILE):
            lo, hi = t * TILE, (t + 1) * TILE
            lefts, rights = [], []
            for i in range(TILE // ROWS):
                left_i, right_i = prepare(t * (TILE // ROWS) + i)
                lefts, rights = lefts + left_i, rights + right_i
            fresh = nn(jnp.concatenate(lefts, axis=1), jnp.concatenate(rights, axis=0))
            known = lane_col < t * (TILE // L_CMP)
            pool_sum[...] = jnp.where(known, pool_sum[...], fresh)
            pooled = pool_sum[...].astype(BF)
            key_pooled = jnp.concatenate([pooled[:HD], jnp.zeros((HD, ROWS), BF)], axis=0)
            val_pooled = pooled[HD:]
            q = q_ext[:, lo:hi].T
            scores = nn(q, k_ext[:, :hi])
            edge = jnp.where(
                iota((TILE, TILE), 1) <= iota((TILE, TILE), 0), scores[:, lo:hi], NEG
            )
            scores = edge if t == 0 else jnp.concatenate([scores[:, :lo], edge], axis=1)
            top = jnp.max(scores, axis=1, keepdims=True)
            e = jnp.exp(scores - top)
            summed = nt(e.astype(BF), v_all[:, :hi])
            picked_out = summed[:, :HD] / summed[:, HD : HD + 1]

            scores = nn(q, key_pooled)
            pos = lo + iota((TILE, ROWS), 0)
            end = iota((TILE, ROWS), 1) * L_CMP + (L_CMP - 1)
            usable = (end <= pos) & (end < length)
            top = jnp.max(jnp.where(usable, scores, NEG), axis=1, keepdims=True)
            e = jnp.where(usable, jnp.exp(jnp.where(usable, scores, NEG) - top), 0.0)
            tot = jnp.sum(e, axis=1, keepdims=True)
            pooled_out = nt(e.astype(BF), val_pooled) / jnp.where(tot > 0, tot, 1.0)

            both = jnp.concatenate([pooled_out, picked_out], axis=1).T
            for i in range(TILE // ROWS):
                j = t * (TILE // ROWS) + i
                g = recv[r, j, EXTRA:MSG, :].astype(F32)
                part = both[:, i * ROWS : (i + 1) * ROWS]
                mix = (g[0:1] + g[2:3]) * part[:HD] + (g[1:2] + g[3:4]) * part[HD:]
                alive = j * ROWS + iota((HD, ROWS), 1) < length
                o_stage[r, j] = jnp.where(alive, mix, 0.0).astype(BF)

                if j not in PAIRED:
                    before = RANK_ORDER[: RANK_ORDER.index(r)]
                    new = [
                        p
                        for p in PLACE[r]
                        if p < j and not any(p in PLACE[q] and j <= LAST[q] for q in before)
                    ]

                    @pl.when(any_of(me, new))
                    def _():
                        pl.semaphore_wait(ready_kv.at[j], 1)

                @pl.when(me != j)
                def _():
                    returned(r, head, j).start()

                @pl.when(me == j)
                def _():
                    a_buf[r, head] = o_stage[r, j]

    for r in RANK_ORDER:

        @pl.when(any_of(me, PLACE[r]))
        def _():
            attend(r)

    half = ROWS // 2
    lower, upper = pl.ds(0, half), pl.ds(half, half)

    def hop(r, block, rows, to, n):
        ref = x_buf.at[r, block] if rows is None else x_buf.at[r, block, rows]
        return pltpu.make_async_remote_copy(
            src_ref=ref,
            dst_ref=ref,
            send_sem=g_send.at[r, n],
            recv_sem=g_recv.at[r, n],
            device_id={"tp": to},
            device_id_type=MESH,
        )

    def sent(r, n):
        return hop(r, *(
            (tp, lower, right, 0),
            (tp, upper, right, 1),
            (tp, upper, left, 2),
            (tp, lower, left, 3),
            (left, lower, right, 4),
            (right, upper, left, 5),
            (tp, None, partner, 6),
            (left, None, partner, 7),
            (right, None, partner, 8),
            (far, None, partner, 9),
        )[n])

    def other(t):
        return t + 1 - 2 * lax.rem(t, 2)

    def received(r, n):
        return hop(r, *(
            (left, lower, left, 0),
            (left, upper, left, 1),
            (right, upper, right, 2),
            (right, lower, right, 3),
            (far, lower, left, 4),
            (far, upper, right, 5),
            (other(tp), None, partner, 6),
            (other(left), None, partner, 7),
            (other(right), None, partner, 8),
            (other(far), None, partner, 9),
        )[n])

    rows_each = ROWS // n_tp
    width = wo.shape[1]

    def column_copy(r, to):
        return pltpu.make_async_remote_copy(
            src_ref=y_buf.at[r, pl.ds(pl.multiple_of(to * rows_each, rows_each), rows_each)],
            dst_ref=o_buf.at[r, :, pl.ds(pl.multiple_of(tp * width, width), width)],
            send_sem=y_send.at[r, to],
            recv_sem=y_recv.at[r, tp],
            device_id={"tp": to},
            device_id_type=MESH,
        )

    def column_arrival(r, source):
        return pltpu.make_async_remote_copy(
            src_ref=y_buf.at[r, pl.ds(0, rows_each)],
            dst_ref=o_buf.at[r, :, pl.ds(pl.multiple_of(source * width, width), width)],
            send_sem=y_send.at[r, source],
            recv_sem=y_recv.at[r, source],
            device_id={"tp": source},
            device_id_type=MESH,
        )

    loads[8].wait()
    for t in range(n_tp):

        @pl.when(tp > t)
        def _():
            pl.semaphore_wait(ready_tp.at[t], 1)


    def own(r):
        for h in range(n_head):

            @pl.when(me != PLACE[r][h])
            def _():
                pltpu.make_async_remote_copy(
                    src_ref=o_stage.at[r, 0],
                    dst_ref=a_buf.at[r, h],
                    send_sem=o_send.at[r, 0],
                    recv_sem=o_recv.at[r, h],
                    device_id={"kv": jnp.int32(PLACE[r][h])},
                    device_id_type=MESH,
                ).wait_recv()

        x_buf[r, tp] = a_buf[r].reshape(n_head * HD, ROWS).T
        for n in (0, 2, 1, 3, 6):
            sent(r, n).start()

    def relay(r):
        received(r, 0).wait_recv()
        sent(r, 4).start()
        received(r, 2).wait_recv()
        sent(r, 5).start()
        received(r, 1).wait_recv()
        sent(r, 7).start()
        received(r, 3).wait_recv()
        sent(r, 8).start()

    def across(r):
        received(r, 4).wait_recv()
        received(r, 5).wait_recv()
        sent(r, 9).start()

    def mix(r):
        for n in (6, 7, 8, 9):
            received(r, n).wait_recv()
        rows = jnp.concatenate([x_buf[r, g] for g in range(n_tp)], axis=1)
        y_buf[r] = nn(rows, wo[...]).astype(BF)
        for step in range(1, n_tp):
            column_copy(r, lax.rem(tp + step, n_tp)).start()
        mine = pl.ds(pl.multiple_of(tp * rows_each, rows_each), rows_each)
        o_buf[r, :, pl.ds(pl.multiple_of(tp * width, width), width)] = y_buf[r, mine]

    def stage(step, r):
        @pl.when(me <= LAST[r])
        def _():
            step(r)

    first, second, third, last = RANK_ORDER
    for step, r in (
        (own, first), (own, second), (relay, first), (own, third), (relay, second),
        (across, first), (relay, third), (across, second), (mix, first), (across, third),
        (mix, second), (mix, third), (own, last), (relay, last), (across, last), (mix, last),
    ):
        stage(step, r)

    for r in range(n_seq):

        @pl.when(me > LAST[r])
        def _():
            o_buf[r] = jnp.zeros(o_buf.shape[1:], BF)

    for r in range(n_seq):

        @pl.when(me <= LAST[r])
        def _():
            for step in range(1, n_tp):
                column_arrival(r, lax.rem(tp + step, n_tp)).wait_recv()

    many = rows_each * n_seq
    want = iota((many, many), 0)
    have = iota((many, many), 1)
    pick = jnp.zeros((many, many), F32)
    for r in range(n_seq):
        hit = (have == r * rows_each + want // n_seq) & (lax.rem(want, n_seq) == seq_of[r])
        pick = jnp.where(hit, 1.0, pick)
    pick = pick.astype(BF)
    for c in range(n_tp):
        cols = slice(c * width, (c + 1) * width)
        rows = o_buf[:, :, cols].reshape(many, width)
        out_ref[:, :, cols] = nn(pick, rows).astype(BF).reshape(rows_each, n_seq, width)

    for r in range(n_seq):
        for h in range(n_head):

            @pl.when((me <= LAST[r]) & (me != PLACE[r][h]))
            def _():
                message(r, h, False).wait_send()
                message(r, h, True).wait_send()

        @pl.when(any_of(me, PLACE[r]))
        def _():
            for j in range(LAST[r] + 1):

                @pl.when(me != j)
                def _():
                    returned(r, 0, j).wait_send()

        @pl.when(me <= LAST[r])
        def _():
            for n in range(10):
                sent(r, n).wait_send()
            for step in range(1, n_tp):
                column_copy(r, lax.rem(tp + step, n_tp)).wait_send()


def body(tokens, lengths, chosen, w_query, w_key, w_value, w_gate, pool_weights, w_out):
    rows, n_seq, depth = tokens.shape
    n_head = w_query.shape[1] // HD
    n_kv, n_tp = lax.axis_size("kv"), lax.axis_size("tp")
    gate_rows = jnp.transpose(w_gate, (1, 2, 0))
    width = w_out.shape[1]
    total = rows * n_seq
    vmem = pl.BlockSpec(memory_space=pltpu.VMEM)
    hbm = pl.BlockSpec(memory_space=pl.ANY)
    dma = pltpu.SemaphoreType.DMA
    full = n_kv * rows

    def whole(*refs):
        kernel(n_kv, n_tp, n_seq, n_head, *refs)

    return pl.pallas_call(
        whole,
        out_shape=jax.ShapeDtypeStruct((rows // n_tp, n_seq, n_tp * width), BF),
        in_specs=[hbm] * 9,
        out_specs=vmem,
        scratch_shapes=[
            pltpu.VMEM((rows, n_seq, depth), BF),
            pltpu.VMEM((total, depth), BF),
            pltpu.VMEM((3, depth, n_head * HD), BF),
            pltpu.VMEM(gate_rows.shape, BF),
            pltpu.VMEM(pool_weights.shape, F32),
            pltpu.VMEM(w_out.shape, BF),
            pltpu.SMEM(lengths.shape, jnp.int32),
            pltpu.SMEM(chosen.shape, jnp.int32),
            pltpu.VMEM((total, total), BF),
            pltpu.VMEM((n_seq * n_head, MSG, rows), BF),
            pltpu.VMEM((n_seq, n_kv, MSG, rows), BF),
            pltpu.VMEM((128, full), BF),
            pltpu.VMEM((128, full), BF),
            pltpu.VMEM((128, full), BF),
            pltpu.VMEM((2 * HD, rows), F32),
            pltpu.VMEM((2 * HD, rows), F32),
            pltpu.VMEM((n_seq, n_kv, HD, rows), BF),
            pltpu.VMEM((n_seq, n_head, HD, rows), BF),
            pltpu.VMEM((n_seq, n_tp, rows, n_head * HD), BF),
            pltpu.VMEM((n_seq, rows, width), BF),
            pltpu.VMEM((n_seq, rows // n_tp, n_tp * width), BF),
            dma((9,)),
            dma((n_seq * n_head,)),
            dma((n_seq, n_kv)),
            dma((n_seq * n_head,)),
            dma((n_seq, n_kv)),
            dma((n_seq, n_kv)),
            dma((n_seq, n_head)),
            dma((n_seq, 10)),
            dma((n_seq, 10)),
            dma((n_seq, n_tp)),
            dma((n_seq, n_tp)),
            pltpu.SemaphoreType.REGULAR((n_kv,)),
            pltpu.SemaphoreType.REGULAR((n_tp,)),
        ],
        compiler_params=pltpu.CompilerParams(
            collective_id=0, has_side_effects=True, vmem_limit_bytes=60 * 2**20
        ),
    )(tokens, lengths, chosen, w_query, w_key, w_value, gate_rows, pool_weights, w_out)


def solution(mesh):
    placed = (
        P("kv", "grp", None),
        P("grp"),
        P("grp", "tp", "kv", None),
        P(None, "tp"),
        P(None, "tp"),
        P(None, "tp"),
        P(None, None, "tp"),
        P(),
        P(None, "tp"),
    )
    return jax.shard_map(
        body, mesh=mesh, in_specs=placed, out_specs=P(("kv", "tp"), "grp", None), check_vma=False
    )
```

time: 115 us -> 87.4 us (0.76)
  Pallas kernels: 109 us -> 85.2 us
  local copies, waits for them, and re-layouts: 4.63 us -> 2.03 us
    pallas_call x1, Pallas kernels: 109 us -> 85.2 us  [body(): pl.pallas_call(whole, out_shape=jax.ShapeDtypeStruct((rows // n_tp, n_seq...]
    reshape x2 -> x0, local copies, waits for them, and re-layouts: 3.51 us -> none  [the longest x1 2.03 us: body(): return out.reshape(rows // n_tp, n_seq, n_tp * width)]
    unnamed x0 -> x1, local copies, waits for them, and re-layouts: none -> 2.03 us
where the time goes in v2:
time: 87.4 us; the launch traced here: 87.2 us
  Pallas kernels  85.2 us (97%)
  local copies, waits for them, and re-layouts  2.03 us (2%)
    pallas_call x1, Pallas kernels, body(): pl.pallas_call(whole, out_shape=jax.ShapeDtypeStruct((rows // n_tp, n_seq...  85.2 us
    unnamed x1, local copies, waits for them, and re-layouts  2.03 us

profile of v2, /device:TPU:33, one launch (start us, length us, event | category | flops | bytes accessed | tf_op | source)
XLA Modules:
  0.0 87.2 jit_solution(4131515678351428634)
XLA Ops:
  0.0 85.2 %shard_map.91 = bf16[16,4,4096]{2,1,0:T(4,128)(2,1)} custom-call(bf16[128,4,4096]{2,1,0:T(4,128)(2,1)} %refs_0_.1, s32[4]{0:T(128)} %refs_1_.1, s32[4,4,2,8]{3,2,1,0:T(2,128)} %refs_2_.1, bf16[4096,256]{1,0:T(8,128)(2,1)} %refs_3_.1, bf16[4096,256]{1,0:T(8,128)(2,1)} %refs_4_.1, bf16[4096,256]{1,0:T(8,128)(2,1)} %refs_5_.1, bf16[2,4,4096]{2,1,0:T(4,128)(2,1)} %bitcast.1, ...), custom_call_target="tpu_custom_call" | custom-call | tf_op jit(solution)/shard_map/pallas_call | solution.py:579
  85.2 2.0 %copy.11 = bf16[16,4,4096]{2,1,0:T(4,128)(2,1)} copy(bf16[16,4,4096]{2,1,0:T(4,128)(2,1)} %shard_map.91) | data formatting | bytes 1048576

commit v3 on v2

--- a/solution.py
+++ b/solution.py
@@ -64,7 +64,7 @@
     out_ref,
     tok, flat, w_buf, wg, pw_ref, wo, len_ref, chosen_ref,
     sel_t, send, recv, k_ext, q_ext, v_all, weight, pool_sum, o_stage, a_buf, x_buf, y_buf, o_buf,
-    load_sem, k_send, k_recv, q_send, q_recv, o_send, o_recv, g_send, g_recv, y_send, y_recv,
+    load_sem, q_send, q_recv, o_send, o_recv, g_send, g_recv, y_send, y_recv,
     ready_kv, ready_tp,
 ):
     me = lax.axis_index("kv")
@@ -199,35 +199,37 @@
                 aux = jnp.concatenate([*kinds, rest, picked.astype(F32)], axis=0)
                 send[r * n_head + h, EXTRA:, :] = aux.astype(BF)
 
-    pair_rows = pl.ds(0, QUER)
-    query_rows = pl.ds(QUER, MSG - QUER)
-
-    def message(r, h, queries):
-        rows = query_rows if queries else pair_rows
+    wholes = ((0, MSG),)
+    halves = ((0, QUER), (QUER, MSG - QUER))
+    thirds = ((KEYS, HD), (VALS, HD), (QUER, MSG - QUER))
+    parts_of = {3: thirds, 2: thirds, 1: halves, 0: wholes}
+
+    def message(r, h, part):
+        rows = pl.ds(*parts_of[r][part])
         return pltpu.make_async_remote_copy(
             src_ref=send.at[r * n_head + h, rows],
             dst_ref=recv.at[r, me, rows],
-            send_sem=(q_send if queries else k_send).at[r * n_head + h],
-            recv_sem=(q_recv if queries else k_recv).at[r, me],
+            send_sem=q_send.at[part, r * n_head + h],
+            recv_sem=q_recv.at[part, r, me],
             device_id={"kv": jnp.int32(PLACE[r][h])},
             device_id_type=MESH,
         )
 
-    def arrival(r, j, queries):
-        rows = query_rows if queries else pair_rows
+    def arrival(r, j, part):
+        rows = pl.ds(*parts_of[r][part])
         return pltpu.make_async_remote_copy(
             src_ref=send.at[0, rows],
             dst_ref=recv.at[r, j, rows],
-            send_sem=(q_send if queries else k_send).at[0],
-            recv_sem=(q_recv if queries else k_recv).at[r, j],
+            send_sem=q_send.at[part, 0],
+            recv_sem=q_recv.at[part, r, j],
             device_id={"kv": jnp.int32(0)},
             device_id_type=MESH,
         )
 
     asked = set()
 
-    def send_rank(r, queries):
-        for h in range(n_head):
+    def send_rank(r, part):
+        for h in sorted(range(n_head), key=lambda h: PLACE[r][h]):
             there = PLACE[r][h]
             if there not in asked:
                 asked.add(there)
@@ -238,25 +240,27 @@
 
             @pl.when((me <= LAST[r]) & (me != there))
             def _():
-                message(r, h, queries).start()
-
-            if queries and there <= LAST[r]:
+                message(r, h, part).start()
+
+            if part == len(parts_of[r]) - 1 and there <= LAST[r]:
 
                 @pl.when(me == there)
                 def _():
                     recv[r, there] = send[r * n_head + h]
 
     project(0, KEYS)
+    send_rank(3, 0)
+    send_rank(2, 0)
     project(1, VALS)
-    for r in RANK_ORDER[:2]:
-        send_rank(r, False)
+    send_rank(3, 1)
+    send_rank(2, 1)
     project(2, QUER)
+    send_rank(1, 0)
     extras()
-    for r in RANK_ORDER[:2]:
-        send_rank(r, True)
-    for r in RANK_ORDER[2:]:
-        send_rank(r, False)
-        send_rank(r, True)
+    send_rank(3, 2)
+    send_rank(2, 2)
+    send_rank(1, 1)
+    send_rank(0, 0)
     loads[7].wait()
 
     def returned(r, h_here, j):
@@ -286,8 +290,8 @@
         def prepare(j):
             @pl.when(me != j)
             def _():
-                arrival(r, j, False).wait_recv()
-                arrival(r, j, True).wait_recv()
+                for part in range(len(parts_of[r])):
+                    arrival(r, j, part).wait_recv()
 
             cols = slice(j * ROWS, (j + 1) * ROWS)
             q_ext[0:HD, cols] = recv[r, j, QUER:EXTRA, :]
@@ -505,9 +509,9 @@
 
     first, second, third, last = RANK_ORDER
     for step, r in (
-        (own, first), (own, second), (relay, first), (own, third), (relay, second),
-        (across, first), (relay, third), (across, second), (mix, first), (across, third),
-        (mix, second), (mix, third), (own, last), (relay, last), (across, last), (mix, last),
+        (own, first), (own, second), (relay, first), (own, third), (relay, second), (own, last),
+        (across, first), (relay, third), (across, second), (mix, first), (relay, last),
+        (across, third), (mix, second), (across, last), (mix, third), (mix, last),
     ):
         stage(step, r)
 
@@ -542,8 +546,8 @@
 
             @pl.when((me <= LAST[r]) & (me != PLACE[r][h]))
             def _():
-                message(r, h, False).wait_send()
-                message(r, h, True).wait_send()
+                for part in range(len(parts_of[r])):
+                    message(r, h, part).wait_send()
 
         @pl.when(any_of(me, PLACE[r]))
         def _():
@@ -604,10 +608,8 @@
             pltpu.VMEM((n_seq, rows, width), BF),
             pltpu.VMEM((n_seq, rows // n_tp, n_tp * width), BF),
             dma((9,)),
-            dma((n_seq * n_head,)),
-            dma((n_seq, n_kv)),
-            dma((n_seq * n_head,)),
-            dma((n_seq, n_kv)),
+            dma((3, n_seq * n_head)),
+            dma((3, n_seq, n_kv)),
             dma((n_seq, n_kv)),
             dma((n_seq, n_head)),
             dma((n_seq, 10)),

time: 87.4 us -> 83.3 us (0.953)
  Pallas kernels: 85.2 us -> 81.1 us
    pallas_call x1, Pallas kernels: 85.2 us -> 81.1 us  [body(): pl.pallas_call(whole, out_shape=jax.ShapeDtypeStruct((rows // n_tp, n_seq...]
where the time goes in v3:
time: 83.3 us; the launch traced here: 83.2 us
  Pallas kernels  81.1 us (97%)
  local copies, waits for them, and re-layouts  2.03 us (2%)
    pallas_call x1, Pallas kernels, body(): pl.pallas_call(whole, out_shape=jax.ShapeDtypeStruct((rows // n_tp, n_seq...  81.1 us
    unnamed x1, local copies, waits for them, and re-layouts  2.03 us

profile of v3, /device:TPU:33, one launch (start us, length us, event | category | flops | bytes accessed | tf_op | source)
XLA Modules:
  0.0 83.2 jit_solution(14346777716466190632)
XLA Ops:
  0.0 81.1 %shard_map.91 = bf16[16,4,4096]{2,1,0:T(4,128)(2,1)} custom-call(bf16[128,4,4096]{2,1,0:T(4,128)(2,1)} %refs_0_.1, s32[4]{0:T(128)} %refs_1_.1, s32[4,4,2,8]{3,2,1,0:T(2,128)} %refs_2_.1, bf16[4096,256]{1,0:T(8,128)(2,1)} %refs_3_.1, bf16[4096,256]{1,0:T(8,128)(2,1)} %refs_4_.1, bf16[4096,256]{1,0:T(8,128)(2,1)} %refs_5_.1, bf16[2,4,4096]{2,1,0:T(4,128)(2,1)} %bitcast.1, ...), custom_call_target="tpu_custom_call" | custom-call | tf_op jit(solution)/shard_map/pallas_call | solution.py:583
  81.1 2.0 %copy.11 = bf16[16,4,4096]{2,1,0:T(4,128)(2,1)} copy(bf16[16,4,4096]{2,1,0:T(4,128)(2,1)} %shard_map.91) | data formatting | bytes 1048576

commit v4 on v3

--- a/solution.py
+++ b/solution.py
@@ -26,6 +26,8 @@
 )
 RANK_ORDER = (3, 2, 1, 0)
 TILE = 256
+AHEAD = 2
+RELAY_SEM = (0, 1, 2, 3, 4, 4, 5, 5, 5, 5)
 SHARDS = LAST[0] + 1
 PAIRED = sorted({p for places in PLACE for p in places})
 
@@ -37,6 +39,9 @@
 def sends_to(i, j):
     asked = any(j in PLACE[r] and i <= LAST[r] for r in range(len(PLACE)))
     return asked or returns_to(i, j)
+
+
+FIRST = [sum(LAST[:r]) + r for r in range(len(LAST))]
 
 
 def any_of(me, places):
@@ -209,22 +214,36 @@
         return pltpu.make_async_remote_copy(
             src_ref=send.at[r * n_head + h, rows],
             dst_ref=recv.at[r, me, rows],
-            send_sem=q_send.at[part, r * n_head + h],
-            recv_sem=q_recv.at[part, r, me],
+            send_sem=q_send.at[r],
+            recv_sem=q_recv.at[FIRST[r] + me],
             device_id={"kv": jnp.int32(PLACE[r][h])},
             device_id_type=MESH,
         )
 
-    def arrival(r, j, part):
-        rows = pl.ds(*parts_of[r][part])
+    def arrival(r, j):
         return pltpu.make_async_remote_copy(
-            src_ref=send.at[0, rows],
-            dst_ref=recv.at[r, j, rows],
-            send_sem=q_send.at[part, 0],
-            recv_sem=q_recv.at[part, r, j],
+            src_ref=send.at[0],
+            dst_ref=recv.at[r, j],
+            send_sem=q_send.at[r],
+            recv_sem=q_recv.at[FIRST[r] + j],
             device_id={"kv": jnp.int32(0)},
             device_id_type=MESH,
         )
+
+    def departures(r, count):
+        return pltpu.make_async_remote_copy(
+            src_ref=send.at[pl.ds(0, count)],
+            dst_ref=send.at[pl.ds(0, count)],
+            send_sem=q_send.at[r],
+            recv_sem=q_recv.at[0],
+            device_id={"kv": jnp.int32(0)},
+            device_id_type=MESH,
+        )
+
+    def await_ready(there):
+        @pl.when(any_of(me, [i for i in range(there) if sends_to(i, there)]))
+        def _():
+            pl.semaphore_wait(ready_kv.at[there], 1)
 
     asked = set()
 
@@ -233,42 +252,71 @@
             there = PLACE[r][h]
             if there not in asked:
                 asked.add(there)
-
-                @pl.when(any_of(me, [i for i in range(there) if sends_to(i, there)]))
-                def _():
-                    pl.semaphore_wait(ready_kv.at[there], 1)
+                await_ready(there)
 
             @pl.when((me <= LAST[r]) & (me != there))
             def _():
                 message(r, h, part).start()
 
-            if part == len(parts_of[r]) - 1 and there <= LAST[r]:
+    ahead = me < AHEAD
+    project(0, KEYS)
+
+    @pl.when(jnp.logical_not(ahead))
+    def _():
+        send_rank(3, 0)
+        send_rank(2, 0)
+
+    project(1, VALS)
+
+    @pl.when(jnp.logical_not(ahead))
+    def _():
+        send_rank(3, 1)
+        send_rank(2, 1)
+
+    project(2, QUER)
+
+    @pl.when(jnp.logical_not(ahead))
+    def _():
+        send_rank(1, 0)
+
+    extras()
+    for r in range(n_seq):
+        for h in range(n_head):
+            there = PLACE[r][h]
+            if there <= LAST[r]:
 
                 @pl.when(me == there)
                 def _():
                     recv[r, there] = send[r * n_head + h]
 
-    project(0, KEYS)
-    send_rank(3, 0)
-    send_rank(2, 0)
-    project(1, VALS)
-    send_rank(3, 1)
-    send_rank(2, 1)
-    project(2, QUER)
-    send_rank(1, 0)
-    extras()
-    send_rank(3, 2)
-    send_rank(2, 2)
-    send_rank(1, 1)
-    send_rank(0, 0)
+    @pl.when(ahead)
+    def _():
+        for there in PAIRED:
+            await_ready(there)
+            for r in (3, 2, 1, 0):
+                for h in range(n_head):
+                    if PLACE[r][h] == there:
+                        for part in range(len(parts_of[r])):
+
+                            @pl.when(me != there)
+                            def _():
+                                message(r, h, part).start()
+
+    @pl.when(jnp.logical_not(ahead))
+    def _():
+        send_rank(3, 2)
+        send_rank(2, 2)
+        send_rank(1, 1)
+        send_rank(0, 0)
+
     loads[7].wait()
 
     def returned(r, h_here, j):
         return pltpu.make_async_remote_copy(
             src_ref=o_stage.at[r, j],
             dst_ref=a_buf.at[r, h_here],
-            send_sem=o_send.at[r, j],
-            recv_sem=o_recv.at[r, h_here],
+            send_sem=o_send.at[r],
+            recv_sem=o_recv.at[r],
             device_id={"kv": jnp.int32(j)},
             device_id_type=MESH,
         )
@@ -290,8 +338,7 @@
         def prepare(j):
             @pl.when(me != j)
             def _():
-                for part in range(len(parts_of[r])):
-                    arrival(r, j, part).wait_recv()
+                arrival(r, j).wait_recv()
 
             cols = slice(j * ROWS, (j + 1) * ROWS)
             q_ext[0:HD, cols] = recv[r, j, QUER:EXTRA, :]
@@ -391,8 +438,8 @@
         return pltpu.make_async_remote_copy(
             src_ref=ref,
             dst_ref=ref,
-            send_sem=g_send.at[r, n],
-            recv_sem=g_recv.at[r, n],
+            send_sem=g_send.at[r],
+            recv_sem=g_recv.at[r, RELAY_SEM[n]],
             device_id={"tp": to},
             device_id_type=MESH,
         )
@@ -435,19 +482,20 @@
         return pltpu.make_async_remote_copy(
             src_ref=y_buf.at[r, pl.ds(pl.multiple_of(to * rows_each, rows_each), rows_each)],
             dst_ref=o_buf.at[r, :, pl.ds(pl.multiple_of(tp * width, width), width)],
-            send_sem=y_send.at[r, to],
-            recv_sem=y_recv.at[r, tp],
+            send_sem=y_send.at[r],
+            recv_sem=y_recv.at[r],
             device_id={"tp": to},
             device_id_type=MESH,
         )
 
-    def column_arrival(r, source):
+    def columns_all(r):
+        rest = pl.ds(0, (n_tp - 1) * rows_each)
         return pltpu.make_async_remote_copy(
-            src_ref=y_buf.at[r, pl.ds(0, rows_each)],
-            dst_ref=o_buf.at[r, :, pl.ds(pl.multiple_of(source * width, width), width)],
-            send_sem=y_send.at[r, source],
-            recv_sem=y_recv.at[r, source],
-            device_id={"tp": source},
+            src_ref=y_buf.at[r, rest],
+            dst_ref=y_buf.at[r, rest],
+            send_sem=y_send.at[r],
+            recv_sem=y_recv.at[r],
+            device_id={"tp": partner},
             device_id_type=MESH,
         )
 
@@ -459,19 +507,26 @@
             pl.semaphore_wait(ready_tp.at[t], 1)
 
 
+    def handed_back(r, count):
+        return pltpu.make_async_remote_copy(
+            src_ref=o_stage.at[r, pl.ds(0, count)],
+            dst_ref=a_buf.at[r, pl.ds(0, count)],
+            send_sem=o_send.at[r],
+            recv_sem=o_recv.at[r],
+            device_id={"kv": jnp.int32(0)},
+            device_id_type=MESH,
+        )
+
     def own(r):
-        for h in range(n_head):
-
-            @pl.when(me != PLACE[r][h])
-            def _():
-                pltpu.make_async_remote_copy(
-                    src_ref=o_stage.at[r, 0],
-                    dst_ref=a_buf.at[r, h],
-                    send_sem=o_send.at[r, 0],
-                    recv_sem=o_recv.at[r, h],
-                    device_id={"kv": jnp.int32(PLACE[r][h])},
-                    device_id_type=MESH,
-                ).wait_recv()
+        inside = any_of(me, PLACE[r])
+
+        @pl.when(inside)
+        def _():
+            handed_back(r, n_head - 1).wait_recv()
+
+        @pl.when(jnp.logical_not(inside))
+        def _():
+            handed_back(r, n_head).wait_recv()
 
         x_buf[r, tp] = a_buf[r].reshape(n_head * HD, ROWS).T
         for n in (0, 2, 1, 3, 6):
@@ -488,13 +543,19 @@
         sent(r, 8).start()
 
     def across(r):
-        received(r, 4).wait_recv()
-        received(r, 5).wait_recv()
+        hop(r, far, None, left, 4).wait_recv()
         sent(r, 9).start()
 
     def mix(r):
-        for n in (6, 7, 8, 9):
-            received(r, n).wait_recv()
+        blocks = x_buf.at[r, pl.ds(0, n_tp // 2)]
+        pltpu.make_async_remote_copy(
+            src_ref=blocks,
+            dst_ref=blocks,
+            send_sem=g_send.at[r],
+            recv_sem=g_recv.at[r, RELAY_SEM[6]],
+            device_id={"tp": partner},
+            device_id_type=MESH,
+        ).wait_recv()
         rows = jnp.concatenate([x_buf[r, g] for g in range(n_tp)], axis=1)
         y_buf[r] = nn(rows, wo[...]).astype(BF)
         for step in range(1, n_tp):
@@ -525,8 +586,7 @@
 
         @pl.when(me <= LAST[r])
         def _():
-            for step in range(1, n_tp):
-                column_arrival(r, lax.rem(tp + step, n_tp)).wait_recv()
+            columns_all(r).wait_recv()
 
     many = rows_each * n_seq
     want = iota((many, many), 0)
@@ -542,27 +602,48 @@
         out_ref[:, :, cols] = nn(pick, rows).astype(BF).reshape(rows_each, n_seq, width)
 
     for r in range(n_seq):
-        for h in range(n_head):
-
-            @pl.when((me <= LAST[r]) & (me != PLACE[r][h]))
+        inside = any_of(me, PLACE[r])
+
+        @pl.when((me <= LAST[r]) & inside)
+        def _():
+            departures(r, n_head - 1).wait_send()
+
+        @pl.when((me <= LAST[r]) & jnp.logical_not(inside))
+        def _():
+            departures(r, n_head).wait_send()
+
+        def returned_all(count):
+            return pltpu.make_async_remote_copy(
+                src_ref=o_stage.at[r, pl.ds(0, count)],
+                dst_ref=o_stage.at[r, pl.ds(0, count)],
+                send_sem=o_send.at[r],
+                recv_sem=o_recv.at[r],
+                device_id={"kv": jnp.int32(0)},
+                device_id_type=MESH,
+            )
+
+        @pl.when(inside & (me <= LAST[r]))
+        def _():
+            returned_all(LAST[r]).wait_send()
+
+        if any(p > LAST[r] for p in PLACE[r]):
+
+            @pl.when(inside & (me > LAST[r]))
             def _():
-                for part in range(len(parts_of[r])):
-                    message(r, h, part).wait_send()
-
-        @pl.when(any_of(me, PLACE[r]))
-        def _():
-            for j in range(LAST[r] + 1):
-
-                @pl.when(me != j)
-                def _():
-                    returned(r, 0, j).wait_send()
+                returned_all(LAST[r] + 1).wait_send()
 
         @pl.when(me <= LAST[r])
         def _():
-            for n in range(10):
-                sent(r, n).wait_send()
-            for step in range(1, n_tp):
-                column_copy(r, lax.rem(tp + step, n_tp)).wait_send()
+            blocks = x_buf.at[r, pl.ds(0, 2 + 1 + n_tp // 2)]
+            pltpu.make_async_remote_copy(
+                src_ref=blocks,
+                dst_ref=blocks,
+                send_sem=g_send.at[r],
+                recv_sem=g_recv.at[r, 0],
+                device_id={"tp": partner},
+                device_id_type=MESH,
+            ).wait_send()
+            columns_all(r).wait_send()
 
 
 def body(tokens, lengths, chosen, w_query, w_key, w_value, w_gate, pool_weights, w_out):
@@ -608,14 +689,14 @@
             pltpu.VMEM((n_seq, rows, width), BF),
             pltpu.VMEM((n_seq, rows // n_tp, n_tp * width), BF),
             dma((9,)),
-            dma((3, n_seq * n_head)),
-            dma((3, n_seq, n_kv)),
-            dma((n_seq, n_kv)),
-            dma((n_seq, n_head)),
-            dma((n_seq, 10)),
-            dma((n_seq, 10)),
-            dma((n_seq, n_tp)),
-            dma((n_seq, n_tp)),
+            dma((n_seq,)),
+            dma((FIRST[-1] + LAST[-1] + 1,)),
+            dma((n_seq,)),
+            dma((n_seq,)),
+            dma((n_seq,)),
+            dma((n_seq, 6)),
+            dma((n_seq,)),
+            dma((n_seq,)),
             pltpu.SemaphoreType.REGULAR((n_kv,)),
             pltpu.SemaphoreType.REGULAR((n_tp,)),
         ],

time: 83.3 us -> 79.7 us (0.957)
  Pallas kernels: 81.1 us -> 77.4 us
    pallas_call x1, Pallas kernels: 81.1 us -> 77.4 us  [body(): pl.pallas_call(whole, out_shape=jax.ShapeDtypeStruct((rows // n_tp, n_seq...]
where the time goes in v4:
time: 79.7 us; the launch traced here: 79.4 us
  Pallas kernels  77.4 us (97%)
  local copies, waits for them, and re-layouts  2.03 us (3%)
    pallas_call x1, Pallas kernels, body(): pl.pallas_call(whole, out_shape=jax.ShapeDtypeStruct((rows // n_tp, n_seq...  77.4 us
    unnamed x1, local copies, waits for them, and re-layouts  2.03 us

profile of v4, /device:TPU:33, one launch (start us, length us, event | category | flops | bytes accessed | tf_op | source)
XLA Modules:
  0.0 79.4 jit_solution(6685079300461551535)
XLA Ops:
  0.0 77.4 %shard_map.91 = bf16[16,4,4096]{2,1,0:T(4,128)(2,1)} custom-call(bf16[128,4,4096]{2,1,0:T(4,128)(2,1)} %refs_0_.1, s32[4]{0:T(128)} %refs_1_.1, s32[4,4,2,8]{3,2,1,0:T(2,128)} %refs_2_.1, bf16[4096,256]{1,0:T(8,128)(2,1)} %refs_3_.1, bf16[4096,256]{1,0:T(8,128)(2,1)} %refs_4_.1, bf16[4096,256]{1,0:T(8,128)(2,1)} %refs_5_.1, bf16[2,4,4096]{2,1,0:T(4,128)(2,1)} %bitcast.1, ...), custom_call_target="tpu_custom_call" | custom-call | tf_op jit(solution)/shard_map/pallas_call | solution.py:664
  77.4 2.0 %copy.11 = bf16[16,4,4096]{2,1,0:T(4,128)(2,1)} copy(bf16[16,4,4096]{2,1,0:T(4,128)(2,1)} %shard_map.91) | data formatting | bytes 1048576

commit v5 on v4

--- a/solution.py
+++ b/solution.py
@@ -27,6 +27,7 @@
 RANK_ORDER = (3, 2, 1, 0)
 TILE = 256
 AHEAD = 2
+NEAR = 4
 RELAY_SEM = (0, 1, 2, 3, 4, 4, 5, 5, 5, 5)
 SHARDS = LAST[0] + 1
 PAIRED = sorted({p for places in PLACE for p in places})
@@ -85,7 +86,14 @@
     barrier = pltpu.get_barrier_semaphore()
     for j in range(n_kv):
 
-        @pl.when(me < j)
+        if j == 0:
+            tells = (me > 0) & (me < NEAR)
+        elif j < NEAR:
+            tells = (me > 0) & (me < j)
+        else:
+            tells = me < j
+
+        @pl.when(tells)
         def _():
             pl.semaphore_signal(
                 barrier, inc=1, device_id={"kv": jnp.int32(j)}, device_id_type=MESH
@@ -112,29 +120,33 @@
     ]
     for copy in loads:
         copy.start()
-    told = me + n_tp - 1 - tp
-
-    @pl.when(told > 0)
-    def _():
-        pl.semaphore_wait(barrier, told)
-
-    for i in range(n_kv):
-        later = [j for j in range(i + 1, n_kv) if sends_to(i, j)]
-
-        @pl.when(any_of(me, later))
-        def _():
-            pl.semaphore_signal(
-                ready_kv.at[me], inc=1, device_id={"kv": jnp.int32(i)}, device_id_type=MESH
-            )
-
-    for t in range(n_tp):
-
-        @pl.when(tp < t)
-        def _():
-            pl.semaphore_signal(
-                ready_tp.at[tp], inc=1, device_id={"tp": jnp.int32(t)}, device_id_type=MESH
-            )
-
+    near = (me > 0) & (me < NEAR)
+    told = me + n_tp - 1 - tp - near.astype(jnp.int32) + (me == 0).astype(jnp.int32) * (NEAR - 1)
+
+    def enter():
+        @pl.when(told > 0)
+        def _():
+            pl.semaphore_wait(barrier, told)
+
+        for i in range(n_kv):
+            first = NEAR if i == 0 else i + 1
+            later = [j for j in range(first, n_kv) if sends_to(i, j)]
+
+            @pl.when(any_of(me, later))
+            def _():
+                pl.semaphore_signal(
+                    ready_kv.at[me], inc=1, device_id={"kv": jnp.int32(i)}, device_id_type=MESH
+                )
+
+        for t in range(n_tp):
+
+            @pl.when(tp < t)
+            def _():
+                pl.semaphore_signal(
+                    ready_tp.at[tp], inc=1, device_id={"tp": jnp.int32(t)}, device_id_type=MESH
+                )
+
+    pl.when(near)(enter)
     loads[0].wait()
 
     lens = [len_ref[s] for s in range(n_seq)]
@@ -241,7 +253,9 @@
         )
 
     def await_ready(there):
-        @pl.when(any_of(me, [i for i in range(there) if sends_to(i, there)]))
+        first = 1 if there < NEAR else 0
+
+        @pl.when(any_of(me, [i for i in range(first, there) if sends_to(i, there)]))
         def _():
             pl.semaphore_wait(ready_kv.at[there], 1)
 
@@ -260,6 +274,7 @@
 
     ahead = me < AHEAD
     project(0, KEYS)
+    pl.when(me >= NEAR)(enter)
 
     @pl.when(jnp.logical_not(ahead))
     def _():
@@ -267,11 +282,29 @@
         send_rank(2, 0)
 
     project(1, VALS)
+    pl.when(me == 0)(enter)
+
+    def send_to(there, wanted):
+        for r in (3, 2, 1, 0):
+            for h in range(n_head):
+                if PLACE[r][h] == there:
+                    for part in wanted(r):
+
+                        @pl.when(me != there)
+                        def _():
+                            message(r, h, part).start()
 
     @pl.when(jnp.logical_not(ahead))
     def _():
         send_rank(3, 1)
         send_rank(2, 1)
+
+    @pl.when(ahead)
+    def _():
+        for there in PAIRED:
+            if there < NEAR:
+                await_ready(there)
+                send_to(there, lambda r: range(len(parts_of[r]) - 1))
 
     project(2, QUER)
 
@@ -292,15 +325,12 @@
     @pl.when(ahead)
     def _():
         for there in PAIRED:
-            await_ready(there)
-            for r in (3, 2, 1, 0):
-                for h in range(n_head):
-                    if PLACE[r][h] == there:
-                        for part in range(len(parts_of[r])):
-
-                            @pl.when(me != there)
-                            def _():
-                                message(r, h, part).start()
+            if there < NEAR:
+                send_to(there, lambda r: [len(parts_of[r]) - 1])
+        for there in PAIRED:
+            if there >= NEAR:
+                await_ready(there)
+                send_to(there, lambda r: range(len(parts_of[r])))
 
     @pl.when(jnp.logical_not(ahead))
     def _():

time: 79.7 us -> 82.1 us (1.030)
  Pallas kernels: 77.4 us -> 80 us
    pallas_call x1, Pallas kernels: 77.4 us -> 80 us  [body(): pl.pallas_call(whole, out_shape=jax.ShapeDtypeStruct((rows // n_tp, n_seq...]
where the time goes in v5:
time: 82.1 us; the launch traced here: 82 us
  Pallas kernels  80 us (97%)
  local copies, waits for them, and re-layouts  2.03 us (2%)
    pallas_call x1, Pallas kernels, body(): pl.pallas_call(whole, out_shape=jax.ShapeDtypeStruct((rows // n_tp, n_seq...  80 us
    unnamed x1, local copies, waits for them, and re-layouts  2.03 us

profile of v5, /device:TPU:33, one launch (start us, length us, event | category | flops | bytes accessed | tf_op | source)
XLA Modules:
  0.0 82.0 jit_solution(1201728220335939730)
XLA Ops:
  0.0 80.0 %shard_map.91 = bf16[16,4,4096]{2,1,0:T(4,128)(2,1)} custom-call(bf16[128,4,4096]{2,1,0:T(4,128)(2,1)} %refs_0_.1, s32[4]{0:T(128)} %refs_1_.1, s32[4,4,2,8]{3,2,1,0:T(2,128)} %refs_2_.1, bf16[4096,256]{1,0:T(8,128)(2,1)} %refs_3_.1, bf16[4096,256]{1,0:T(8,128)(2,1)} %refs_4_.1, bf16[4096,256]{1,0:T(8,128)(2,1)} %refs_5_.1, bf16[2,4,4096]{2,1,0:T(4,128)(2,1)} %bitcast.1, ...), custom_call_target="tpu_custom_call" | custom-call | tf_op jit(solution)/shard_map/pallas_call | solution.py:694
  80.0 2.0 %copy.11 = bf16[16,4,4096]{2,1,0:T(4,128)(2,1)} copy(bf16[16,4,4096]{2,1,0:T(4,128)(2,1)} %shard_map.91) | data formatting | bytes 1048576

commit v6 on v5

--- a/solution.py
+++ b/solution.py
@@ -26,8 +26,9 @@
 )
 RANK_ORDER = (3, 2, 1, 0)
 TILE = 256
-AHEAD = 2
-NEAR = 4
+AHEAD = 4
+MIDDLE = (4, 5)
+NEAR = 8
 RELAY_SEM = (0, 1, 2, 3, 4, 4, 5, 5, 5, 5)
 SHARDS = LAST[0] + 1
 PAIRED = sorted({p for places in PLACE for p in places})
@@ -146,7 +147,7 @@
                     ready_tp.at[tp], inc=1, device_id={"tp": jnp.int32(t)}, device_id_type=MESH
                 )
 
-    pl.when(near)(enter)
+    pl.when(me > 0)(enter)
     loads[0].wait()
 
     lens = [len_ref[s] for s in range(n_seq)]
@@ -273,8 +274,8 @@
                 message(r, h, part).start()
 
     ahead = me < AHEAD
+    early = (me > 0) & ahead
     project(0, KEYS)
-    pl.when(me >= NEAR)(enter)
 
     @pl.when(jnp.logical_not(ahead))
     def _():
@@ -282,7 +283,6 @@
         send_rank(2, 0)
 
     project(1, VALS)
-    pl.when(me == 0)(enter)
 
     def send_to(there, wanted):
         for r in (3, 2, 1, 0):
@@ -299,18 +299,35 @@
         send_rank(3, 1)
         send_rank(2, 1)
 
-    @pl.when(ahead)
+    def but_last(r):
+        return range(len(parts_of[r]) - 1)
+
+    def only_last(r):
+        return [len(parts_of[r]) - 1]
+
+    def every(r):
+        return range(len(parts_of[r]))
+
+    near_by = [p for p in PAIRED if p < MIDDLE[0]]
+    beyond = [p for p in PAIRED if p > MIDDLE[-1]]
+
+    @pl.when(early)
     def _():
-        for there in PAIRED:
-            if there < NEAR:
-                await_ready(there)
-                send_to(there, lambda r: range(len(parts_of[r]) - 1))
+        for there in near_by:
+            await_ready(there)
+            send_to(there, but_last)
 
     project(2, QUER)
 
     @pl.when(jnp.logical_not(ahead))
     def _():
         send_rank(1, 0)
+
+    @pl.when(early)
+    def _():
+        for there in MIDDLE:
+            await_ready(there)
+            send_to(there, but_last)
 
     extras()
     for r in range(n_seq):
@@ -322,15 +339,23 @@
                 def _():
                     recv[r, there] = send[r * n_head + h]
 
-    @pl.when(ahead)
+    @pl.when(early)
     def _():
-        for there in PAIRED:
-            if there < NEAR:
-                send_to(there, lambda r: [len(parts_of[r]) - 1])
-        for there in PAIRED:
+        for there in (*near_by, *MIDDLE):
+            send_to(there, only_last)
+        for there in beyond:
+            await_ready(there)
+            send_to(there, every)
+
+    @pl.when(me == 0)
+    def _():
+        enter()
+        for there in [p for p in PAIRED if MIDDLE[0] <= p < NEAR] + near_by:
+            send_to(there, every)
+        for there in beyond:
             if there >= NEAR:
                 await_ready(there)
-                send_to(there, lambda r: range(len(parts_of[r])))
+                send_to(there, every)
 
     @pl.when(jnp.logical_not(ahead))
     def _():

time: 82.1 us -> 76.9 us (0.937)
  the two profiles are of different devices: /device:TPU:33 before, /device:TPU:297 now
where the time goes in v6:
time: 76.9 us; the launch traced here: 76.8 us
  Pallas kernels  74.8 us (97%)
  local copies, waits for them, and re-layouts  2.03 us (3%)
    pallas_call x1, Pallas kernels, body(): pl.pallas_call(whole, out_shape=jax.ShapeDtypeStruct((rows // n_tp, n_seq...  74.8 us
    unnamed x1, local copies, waits for them, and re-layouts  2.03 us

profile of v6, /device:TPU:297, one launch (start us, length us, event | category | flops | bytes accessed | tf_op | source)
XLA Modules:
  0.0 76.8 jit_solution(5805596022461984981)
XLA Ops:
  0.0 74.8 %shard_map.91 = bf16[16,4,4096]{2,1,0:T(4,128)(2,1)} custom-call(bf16[128,4,4096]{2,1,0:T(4,128)(2,1)} %refs_0_.1, s32[4]{0:T(128)} %refs_1_.1, s32[4,4,2,8]{3,2,1,0:T(2,128)} %refs_2_.1, bf16[4096,256]{1,0:T(8,128)(2,1)} %refs_3_.1, bf16[4096,256]{1,0:T(8,128)(2,1)} %refs_4_.1, bf16[4096,256]{1,0:T(8,128)(2,1)} %refs_5_.1, bf16[2,4,4096]{2,1,0:T(4,128)(2,1)} %bitcast.1, ...), custom_call_target="tpu_custom_call" | custom-call | tf_op jit(solution)/shard_map/pallas_call | solution.py:719
  74.8 2.0 %copy.11 = bf16[16,4,4096]{2,1,0:T(4,128)(2,1)} copy(bf16[16,4,4096]{2,1,0:T(4,128)(2,1)} %shard_map.91) | data formatting | bytes 1048576

commit v7 on v6

--- a/solution.py
+++ b/solution.py
@@ -24,7 +24,7 @@
     (3, 4, 1, 2),
     (2, 3, 1, 5),
 )
-RANK_ORDER = (3, 2, 1, 0)
+RANK_ORDER = (1, 2, 3, 0)
 TILE = 256
 AHEAD = 4
 MIDDLE = (4, 5)

time: 76.9 us -> 82.1 us (1.068)
  the two profiles are of different devices: /device:TPU:297 before, /device:TPU:33 now
where the time goes in v7:
time: 82.1 us; the launch traced here: 82 us
  Pallas kernels  79.9 us (97%)
  local copies, waits for them, and re-layouts  2.03 us (2%)
    pallas_call x1, Pallas kernels, body(): pl.pallas_call(whole, out_shape=jax.ShapeDtypeStruct((rows // n_tp, n_seq...  79.9 us
    unnamed x1, local copies, waits for them, and re-layouts  2.03 us

profile of v7, /device:TPU:33, one launch (start us, length us, event | category | flops | bytes accessed | tf_op | source)
XLA Modules:
  0.0 82.0 jit_solution(750197601519041205)
XLA Ops:
  0.0 79.9 %shard_map.91 = bf16[16,4,4096]{2,1,0:T(4,128)(2,1)} custom-call(bf16[128,4,4096]{2,1,0:T(4,128)(2,1)} %refs_0_.1, s32[4]{0:T(128)} %refs_1_.1, s32[4,4,2,8]{3,2,1,0:T(2,128)} %refs_2_.1, bf16[4096,256]{1,0:T(8,128)(2,1)} %refs_3_.1, bf16[4096,256]{1,0:T(8,128)(2,1)} %refs_4_.1, bf16[4096,256]{1,0:T(8,128)(2,1)} %refs_5_.1, bf16[2,4,4096]{2,1,0:T(4,128)(2,1)} %bitcast.1, ...), custom_call_target="tpu_custom_call" | custom-call | tf_op jit(solution)/shard_map/pallas_call | solution.py:719
  79.9 2.0 %copy.11 = bf16[16,4,4096]{2,1,0:T(4,128)(2,1)} copy(bf16[16,4,4096]{2,1,0:T(4,128)(2,1)} %shard_map.91) | data formatting | bytes 1048576
